TPU v7x, 32 devices: a whole 2x2x4 slice. The times are simulated.
32 devices in a mesh: rep: 2 (over y), fs: 4 (over z), tp: 4 (over x, core).
Axes of the slice: x: 2, y: 2, z: 4, core: 2. Of those that a mesh axis runs over, the one named last changes fastest.
Arguments:
- stream: bfloat16 [4096, 2048], P(('rep', 'fs'), 'tp'), parts along dimension 0, may hold values from -6 to 6
- in_weight: bfloat16 [2048, 1024], P('fs', 'tp'), may hold values from -0.125 to 0.125
- pool_weight: bfloat16 [8, 128, 128], P('tp'), may hold values from -0.5 to 0.5
- pool_scale: bfloat16 [1024], P('tp'), may hold values from 0.099609375 to 1.8984375
- out_weight: bfloat16 [1024, 2048], P('tp', 'fs'), may hold values from -0.1875 to 0.1875
- mix_gain: bfloat16 [2048], replicated, may hold values from 0.099609375 to 1.8984375
- ffn_gain: bfloat16 [2048], replicated, may hold values from 0.099609375 to 1.8984375
- gate_weight: bfloat16 [2048, 5632], P('fs', 'tp'), may hold values from -0.125 to 0.125
- up_weight: bfloat16 [2048, 5632], P('fs', 'tp'), may hold values from -0.125 to 0.125
- down_weight: bfloat16 [5632, 2048], P('tp', 'fs'), may hold values from -0.078125 to 0.078125
Outputs:
- result: bfloat16 [4096, 2048], P(('rep', 'fs'), 'tp'), parts along dimension 0
There are 2 independent parts, one for each index of `rep`. A program takes and returns all parts, laid end to end along the dimension named above; an argument that names none is the same for every part. Nothing has to cross between parts.
All inputs are finite; a program needn't handle non-finite values.
Results may differ from a plain program's by a relative error of at most 0.015.
Values may be sent and summed in bfloat16 or wider, within the bound.
A program may use at most 64 MiB of HBM per device.

v0:
```python
import functools

import jax
import jax.numpy as jnp
from jax import lax
from jax.experimental import pallas as pl
from jax.experimental.pallas import tpu as pltpu
from jax.sharding import PartitionSpec as P

SEQ = 128
EPSILON = 1e-06
MESH = pl.DeviceIdType.MESH
BY_ROWS = (True, False, True, True, False)
PIECES = ((0, 0), (1, 0), (2, 0), (3, 0), (2, 1), (3, 1), (4, 0), (4, 1))
CHUNKS = (1, 1, 2, 2, 2)


def kernel(sizes, stream, in_w, out_w, up_w, gate_w, down_w, pool_w, scale,
           mix_gain, ffn_gain, result,
           in_all, out_all, up_all, gate_all, down_all,
           rows_all, normed, group_out, hidden, middle, mid_all,
           mix_send, mix_recv, ffn_send, ffn_recv,
           ring_send, ring_recv, fwd_send, fwd_recv, own_sem,
           tp_send, tp_recv, keep_sem):
    reps, fs, tp = sizes
    half = fs // 2
    my_rep, me, my_tp = lax.axis_index("rep"), lax.axis_index("fs"), lax.axis_index("tp")
    own = (in_w, out_w, up_w, gate_w, down_w)
    full = (in_all, out_all, up_all, gate_all, down_all)
    tokens, width = stream.shape

    def turn(at, by, count):
        return lax.rem(at + by + count, count)

    def piece(which, owner, row, count):
        block_rows, block_cols = own[which].shape
        if BY_ROWS[which]:
            return full[which].at[pl.ds(pl.multiple_of(owner * block_rows + row, 16), count), :]
        return full[which].at[pl.ds(pl.multiple_of(row, 16), count),
                              pl.ds(pl.multiple_of(owner * block_cols, 128), block_cols)]

    def span(number, step, way):
        which, chunk = PIECES[number]
        rows = own[which].shape[0]
        cut = rows % (CHUNKS[which] * reps * 2 * 16) == 0
        count = rows // CHUNKS[which] if cut else (rows, 0)[chunk]
        row = chunk * (rows // CHUNKS[which])
        count = count // reps
        row = row + my_rep * count
        if step == half:
            count = count // 2
            row = row + way * count
        return which, row, count

    def empty(number):
        return span(number, 1, 0)[2] == 0

    def ring(number, step, way):
        which, row, count = span(number, step, way)
        sign = 1 - 2 * way
        owner = turn(me, -sign * (step - 1), fs)
        if step == 1:
            source = own[which].at[pl.ds(pl.multiple_of(row, 16), count), :]
        else:
            source = piece(which, owner, row, count)
        return pltpu.make_async_remote_copy(
            src_ref=source, dst_ref=piece(which, owner, row, count),
            send_sem=ring_send.at[number, step - 1, way],
            recv_sem=ring_recv.at[number, step - 1, way],
            device_id={"fs": turn(me, sign, fs)}, device_id_type=MESH)

    def forward(number, step, way, peer):
        which, row, count = span(number, step, way)
        block = piece(which, turn(me, -(1 - 2 * way) * step, fs), row, count)
        return pltpu.make_async_remote_copy(
            src_ref=block, dst_ref=block,
            send_sem=fwd_send.at[number, peer - 1, step - 1, way],
            recv_sem=fwd_recv.at[number, peer - 1, step - 1, way],
            device_id={"rep": turn(my_rep, peer, reps)}, device_id_type=MESH)

    def begin(*numbers):
        for number in numbers:
            if not empty(number):
                for way in (0, 1):
                    ring(number, 1, way).start()

    def advance(number, step):
        if empty(number):
            return
        for way in (0, 1):
            ring(number, step, way).wait_recv()
            if step < half:
                ring(number, step + 1, way).start()
            for peer in range(1, reps):
                forward(number, step, way, peer).start()

    def early(*numbers):
        for number in numbers:
            for step in range(1, half):
                advance(number, step)

    def late(*numbers):
        for number in numbers:
            advance(number, half)

    def arrived(*numbers):
        for number in numbers:
            if PIECES[number][1] == 0:
                keeps[PIECES[number][0]].wait()
            if empty(number):
                continue
            for step in range(1, half + 1):
                for way in (0, 1):
                    for peer in range(1, reps):
                        forward(number, step, way, peer).wait()

    def tp_copy(stage, offset, source, target):
        return pltpu.make_async_remote_copy(
            src_ref=source, dst_ref=target,
            send_sem=tp_send.at[stage, offset - 1], recv_sem=tp_recv.at[stage, offset - 1],
            device_id={"tp": turn(my_tp, offset, tp)}, device_id_type=MESH)

    def feature_cols(owner):
        return pl.ds(pl.multiple_of(owner * width, 128), width)

    barrier = pltpu.get_barrier_semaphore()
    greeted = 0
    for name, at, count, offsets in (
            ("fs", me, fs, (1, -1)),
            ("tp", my_tp, tp, range(1, tp)),
            ("rep", my_rep, reps, range(1, reps))):
        for offset in offsets:
            pl.semaphore_signal(barrier, inc=1, device_id={name: turn(at, offset, count)},
                                device_id_type=MESH)
            greeted += 1
    pl.semaphore_wait(barrier, greeted)

    begin(0, 1)
    stream_sends = []
    for offset in range(1, tp):
        copy = tp_copy(0, offset, stream, rows_all.at[:, feature_cols(my_tp)])
        copy.start()
        stream_sends.append(copy)
    keeps = []
    for which in range(len(own)):
        keep = pltpu.make_async_copy(
            own[which], piece(which, me, 0, own[which].shape[0]), own_sem.at[which])
        keep.start()
        keeps.append(keep)
    keep_stream = pltpu.make_async_copy(
        stream, rows_all.at[:, feature_cols(my_tp)], keep_sem)
    keep_stream.start()
    early(0, 1)
    begin(2, 3, 4)
    late(0, 1)

    def norm_into(source, gain, target):
        tile = 64

        def body(i, carry):
            at = pl.ds(pl.multiple_of(i * tile, tile), tile)
            wide = source[at, :].astype(jnp.float32)
            mean = jnp.mean(wide * wide, axis=-1, keepdims=True)
            target[at, :] = (wide * lax.rsqrt(mean + EPSILON)
                             * gain[...].astype(jnp.float32)).astype(jnp.bfloat16)
            return carry

        lax.fori_loop(0, tokens // tile, body, 0)

    keep_stream.wait()
    for copy in stream_sends:
        copy.wait()
    norm_into(rows_all, mix_gain, normed)
    arrived(0)

    local_groups, group_dim = pool_w.shape[0], pool_w.shape[1]
    at_row = lax.broadcasted_iota(jnp.int32, (SEQ, SEQ), 0)
    at_col = lax.broadcasted_iota(jnp.int32, (SEQ, SEQ), 1)
    insides, inverses = [], []
    for g in range(local_groups):
        group = my_tp * local_groups + g
        level = lax.div(4 * group, local_groups * tp)
        reach = jnp.int32(2)
        for bit in range(1, 4):
            reach = jnp.where(level >= bit, jnp.int32(2 << bit), reach)
        inside = (at_col <= at_row) & (at_col > at_row - reach)
        insides.append(jnp.where(inside, 1.0, 0.0).astype(jnp.bfloat16))
        inverses.append(jnp.minimum(at_row + 1, reach).astype(jnp.float32)[:, :1])

    def mix(i, carry):
        at = pl.ds(pl.multiple_of(i * SEQ, SEQ), SEQ)
        pooled = jnp.dot(normed[at, :], in_all[...],
                         preferred_element_type=jnp.float32).astype(jnp.bfloat16)
        for g in range(local_groups):
            cols = slice(g * group_dim, (g + 1) * group_dim)
            part = pooled[:, cols]
            sums = jnp.dot(insides[g], part, preferred_element_type=jnp.float32)
            contrast = (sums / inverses[g] - part.astype(jnp.float32)).astype(jnp.bfloat16)
            mixed = jnp.dot(contrast, pool_w[g], preferred_element_type=jnp.float32)
            group_out[at, cols] = (mixed * scale[:, cols].astype(jnp.float32)).astype(jnp.bfloat16)
        return carry

    lax.fori_loop(0, tokens // SEQ, mix, 0)

    arrived(1)
    early(2)

    def spread(operand, weights, stage, sends, tile):
        def block(owner, target):
            def body(i, carry):
                at = pl.ds(pl.multiple_of(i * tile, tile), tile)
                target[at, :] = jnp.dot(operand[at, :], weights[:, feature_cols(owner)],
                                        preferred_element_type=jnp.float32).astype(jnp.bfloat16)
                return carry
            lax.fori_loop(0, tokens // tile, body, 0)

        copies = []
        recv = mix_recv if stage == 1 else ffn_recv
        for offset in sorted(range(1, tp), key=lambda o: -min(o, tp - o)):
            block(turn(my_tp, offset, tp), sends.at[offset - 1])
            copy = tp_copy(stage, offset, sends.at[offset - 1], recv.at[offset - 1])
            copy.start()
            copies.append(copy)
        block(my_tp, sends.at[tp - 1])
        return copies

    def gather_sum(base, recv, sends, target):
        tile = 64

        def body(i, carry):
            at = pl.ds(pl.multiple_of(i * tile, tile), tile)
            total = sends[tp - 1, at, :].astype(jnp.float32)
            for k in range(tp - 1):
                total = total + recv[k, at, :].astype(jnp.float32)
            target[at, :] = (base[at, :].astype(jnp.float32) + total).astype(jnp.bfloat16)
            return carry

        lax.fori_loop(0, tokens // tile, body, 0)

    mix_copies = spread(group_out, out_all, 1, mix_send, tokens // 2)
    early(3)
    begin(5)
    for copy in mix_copies:
        copy.wait()
    gather_sum(stream, mix_recv, mix_send, middle)
    keep_middle = pltpu.make_async_copy(middle, mid_all.at[:, feature_cols(my_tp)], keep_sem)
    keep_middle.start()
    middle_copies = []
    for offset in range(1, tp):
        copy = tp_copy(2, offset, middle, mid_all.at[:, feature_cols(my_tp)])
        copy.start()
        middle_copies.append(copy)
    early(4)
    begin(6, 7)
    late(2, 3)
    keep_middle.wait()
    for copy in middle_copies:
        copy.wait()
    norm_into(mid_all, ffn_gain, normed)
    early(5)
    late(4)
    early(6)
    late(5)
    early(7)
    late(6)
    arrived(2, 3, 4, 5)
    tile = tokens // 2

    def gated(i, carry):
        at = pl.ds(pl.multiple_of(i * tile, tile), tile)
        values = normed[at, :]
        gate = jnp.dot(values, gate_all[...], preferred_element_type=jnp.float32)
        up = jnp.dot(values, up_all[...], preferred_element_type=jnp.float32)
        hidden[at, :] = (gate / (1.0 + jnp.exp(-gate)) * up).astype(jnp.bfloat16)
        return carry

    lax.fori_loop(0, tokens // tile, gated, 0)
    late(7)
    arrived(6, 7)
    ffn_copies = spread(hidden, down_all, 3, ffn_send, tokens // 2)
    for number in range(len(PIECES)):
        if not empty(number):
            for step in range(1, half + 1):
                for way in (0, 1):
                    ring(number, step, way).wait_send()
    for copy in ffn_copies:
        copy.wait()
    gather_sum(middle, ffn_recv, ffn_send, result)


def on_device(sizes, stream, in_weight, pool_weight, pool_scale, out_weight,
              mix_gain, ffn_gain, gate_weight, up_weight, down_weight):
    reps, fs, tp = sizes
    half = fs // 2
    tokens, width = stream.shape
    features = width * tp
    own = (in_weight, out_weight, up_weight, gate_weight, down_weight)
    full = [pltpu.VMEM((w.shape[0] * fs, w.shape[1]) if by_rows else (w.shape[0], w.shape[1] * fs),
                       jnp.bfloat16) for w, by_rows in zip(own, BY_ROWS)]
    units = gate_weight.shape[1]
    bf = jnp.bfloat16
    vmem = pl.BlockSpec(memory_space=pltpu.VMEM)
    hbm = pl.BlockSpec(memory_space=pl.ANY)
    dma = pltpu.SemaphoreType.DMA
    flops = 2 * tokens * (2 * features * in_weight.shape[1] + 3 * features * units)
    return pl.pallas_call(
        functools.partial(kernel, sizes),
        out_shape=jax.ShapeDtypeStruct(stream.shape, bf),
        in_specs=[vmem] + [hbm] * 5 + [vmem] * 4,
        out_specs=vmem,
        scratch_shapes=full + [
            pltpu.VMEM((tokens, features), bf),
            pltpu.VMEM((tokens, features), bf),
            pltpu.VMEM((tokens, in_weight.shape[1]), bf),
            pltpu.VMEM((tokens, units), bf),
            pltpu.VMEM((tokens, width), bf),
            pltpu.VMEM((tokens, features), bf),
            pltpu.VMEM((tp, tokens, width), bf),
            pltpu.VMEM((tp - 1, tokens, width), bf),
            pltpu.VMEM((tp, tokens, width), bf),
            pltpu.VMEM((tp - 1, tokens, width), bf),
            dma((len(PIECES), half, 2)),
            dma((len(PIECES), half, 2)),
            dma((len(PIECES), max(reps - 1, 1), half, 2)),
            dma((len(PIECES), max(reps - 1, 1), half, 2)),
            dma((len(own),)),
            dma((4, tp - 1)),
            dma((4, tp - 1)),
            dma(()),
        ],
        compiler_params=pltpu.CompilerParams(
            collective_id=0, has_side_effects=True, vmem_limit_bytes=64 * 1024 * 1024 - 65536),
        cost_estimate=pl.CostEstimate(flops=flops, bytes_accessed=flops // 512, transcendentals=0),
    )(stream, in_weight, out_weight, up_weight, gate_weight, down_weight, pool_weight,
      pool_scale.reshape(1, -1), mix_gain.reshape(1, -1), ffn_gain.reshape(1, -1))


def solution(mesh):
    sizes = tuple(mesh.shape[name] for name in ("rep", "fs", "tp"))
    return jax.shard_map(
        functools.partial(on_device, sizes),
        mesh=mesh,
        in_specs=(
            P(("rep", "fs"), "tp"),
            P("fs", "tp"),
            P("tp", None, None),
            P("tp"),
            P("tp", "fs"),
            P(),
            P(),
            P("fs", "tp"),
            P("fs", "tp"),
            P("tp", "fs"),
        ),
        out_specs=P(("rep", "fs"), "tp"),
        check_vma=False,
    )
```

profile of v0, /device:TPU:17, one launch (start us, length us, event | category | flops | bytes accessed | tf_op | source)
XLA Modules:
  0.0 213.0 jit_solution(5617818154700964250)
XLA Ops:
  0.0 1.2 reshape.9.scale
  1.2 1.3 reshape.10.mix_gain
  2.5 1.3 reshape.11.ffn_gain
  3.8 207.3 %shard_map.100 = bf16[512,512]{1,0:T(8,128)(2,1)} custom-call(bf16[512,512]{1,0:T(8,128)(2,1)} %stream.1, bf16[512,256]{1,0:T(8,128)(2,1)} %in_w.1, bf16[256,512]{1,0:T(8,128)(2,1)} %out_w.1, bf16[512,1408]{1,0:T(8,128)(2,1)} %up_w.1, bf16[512,1408]{1,0:T(8,128)(2,1)} %gate_w.1, bf16[1408,512]{1,0:T(8,128)(2,1)} %down_w.1, bf16[2,128,128]{2,1,0:T(8,128)(2,1)} %pool_w.1, ...), custom_call_target="tpu_custom_call" | custom-call | flops 9932111872 | bytes 19398656 | tf_op jit(solution)/shard_map/pallas_call | solution.py:306
  211.1 1.9 copy.12
where the time goes:
time: 217 us; the launch traced here: 213 us
  Pallas kernels  207 us (95%)
  local copies, waits for them, and re-layouts  5.64 us (3%)
    pallas_call x1, Pallas kernels, on_device(): pl.pallas_call(functools.partial(kernel, sizes), out_shape=jax.ShapeDtype...  207 us

commit v1 on v0

--- a/solution.py
+++ b/solution.py
@@ -15,7 +15,7 @@
 CHUNKS = (1, 1, 2, 2, 2)
 
 
-def kernel(sizes, stream, in_w, out_w, up_w, gate_w, down_w, pool_w, scale,
+def ring_kernel(sizes, stream, in_w, out_w, up_w, gate_w, down_w, pool_w, scale,
            mix_gain, ffn_gain, result,
            in_all, out_all, up_all, gate_all, down_all,
            rows_all, normed, group_out, hidden, middle, mid_all,
@@ -288,7 +288,7 @@
     gather_sum(middle, ffn_recv, ffn_send, result)
 
 
-def on_device(sizes, stream, in_weight, pool_weight, pool_scale, out_weight,
+def ring_on_device(sizes, stream, in_weight, pool_weight, pool_scale, out_weight,
               mix_gain, ffn_gain, gate_weight, up_weight, down_weight):
     reps, fs, tp = sizes
     half = fs // 2
@@ -304,7 +304,7 @@
     dma = pltpu.SemaphoreType.DMA
     flops = 2 * tokens * (2 * features * in_weight.shape[1] + 3 * features * units)
     return pl.pallas_call(
-        functools.partial(kernel, sizes),
+        functools.partial(ring_kernel, sizes),
         out_shape=jax.ShapeDtypeStruct(stream.shape, bf),
         in_specs=[vmem] + [hbm] * 5 + [vmem] * 4,
         out_specs=vmem,
@@ -335,10 +335,570 @@
       pool_scale.reshape(1, -1), mix_gain.reshape(1, -1), ffn_gain.reshape(1, -1))
 
 
+IN, OUT, UP, GATE, DOWN = range(5)
+LANES = 128
+
+
+def pair_kernel(sizes, stream, in_w, out_w, up_w, gate_w, down_w, pool_w, scale,
+                mix_gain, ffn_gain, result,
+                in_all, out_all, up_all, gate_all, down_all,
+                rows_all, normed, group_out, hidden, mid_all, normed_ffn,
+                pool_sib, scale_sib,
+                mix_own, mix_send, mix_recv, ffn_own, ffn_send, ffn_recv, pair_send, pair_recv,
+                last_send, last_recv,
+                z_send, z_recv, pass_send, y_send, y_recv, d_send, d_recv, own_sem,
+                in_send, in_recv, pool_send, pool_recv, mix_sems, mid_send, mid_recv,
+                x_send, x_recv, p_send, p_recv, l_send, l_recv):
+    reps, fs, tp = sizes
+    y, z, lane_id = lax.axis_index("rep"), lax.axis_index("fs"), lax.axis_index("tp")
+    x, core = lax.div(lane_id, 2), lax.rem(lane_id, 2)
+    own = (in_w, out_w, up_w, gate_w, down_w)
+    full = (in_all, out_all, up_all, gate_all, down_all)
+    tokens, width = stream.shape
+    rows = tokens // 2
+    wide = 2 * width
+    seat, pair = lax.rem(z, 2), lax.div(z, 2)
+    peer = z + 1 - 2 * seat
+    near = jnp.where(pair == 0, 2, 1)
+    far = jnp.where(pair == 0, 3, 0)
+    inner = (z == 1) | (z == 2)
+    f32, bf16 = jnp.float32, jnp.bfloat16
+
+    blocks = gate_w.shape[1] // LANES
+    few, many = blocks // 2, blocks - blocks // 2
+
+    SIB = {"tp": lane_id + 1 - 2 * core}
+    XPEER = {"tp": lane_id + 2 - 4 * x}
+    XSIB = {"tp": 2 * (1 - x) + 1 - core}
+    YPEER = {"rep": 1 - y}
+    ZPEER = {"fs": peer}
+
+    def at_least(value, multiple):
+        return pl.multiple_of(value, multiple)
+
+    def remote(source, target, send, recv, device):
+        return pltpu.make_async_remote_copy(
+            src_ref=source, dst_ref=target, send_sem=send, recv_sem=recv,
+            device_id=device, device_id_type=MESH)
+
+    def sized(which, core_at, seat_at, act):
+        if which in (IN, OUT) or few == many:
+            act(many)
+            return
+        big = core_at == seat_at
+
+        @pl.when(big)
+        def _():
+            act(many)
+
+        @pl.when(jnp.logical_not(big))
+        def _():
+            act(few)
+
+    def place(which, source, half, core_at, seat_at, count):
+        block_rows, block_cols = own[which].shape
+        ref = full[which]
+        if which == IN:
+            part = block_rows // 2
+            row, size = (source * block_rows, block_rows) if half is None else (
+                source * block_rows + half * part, part)
+            return ref.at[pl.ds(at_least(row, 16), size),
+                          pl.ds(at_least(core_at * block_cols, LANES), block_cols)]
+        if which == OUT:
+            part = block_rows // 2
+            row, size = (core_at * block_rows, block_rows) if half is None else (
+                core_at * block_rows + half * part, part)
+            return ref.at[pl.ds(at_least(row, 16), size),
+                          pl.ds(at_least(source * block_cols, LANES), block_cols)]
+        first = core_at * jnp.where(seat_at == 0, many, few) * LANES
+        if which == DOWN:
+            part = block_cols // 2
+            col, size = (source * block_cols, block_cols) if half is None else (
+                source * block_cols + half * part, part)
+            return ref.at[pl.ds(at_least(first, LANES), count * LANES),
+                          pl.ds(at_least(col, LANES), size)]
+        part = block_rows // 2
+        row, size = (source * block_rows, block_rows) if half is None else (
+            source * block_rows + half * part, part)
+        return ref.at[pl.ds(at_least(row, 16), size),
+                      pl.ds(at_least(first, LANES), count * LANES)]
+
+    def held(which, half, seat_at, count):
+        block_rows, block_cols = own[which].shape
+        ref = own[which]
+        if which in (IN, OUT):
+            if half is None:
+                return ref
+            part = block_rows // 2
+            return ref.at[pl.ds(at_least(half * part, 16), part), :]
+        first = seat_at * jnp.where(core == 0, many, few) * LANES
+        if which == DOWN:
+            part = block_cols // 2
+            unit_rows = pl.ds(at_least(first, LANES), count * LANES)
+            if half is None:
+                return ref.at[unit_rows, :]
+            return ref.at[unit_rows, pl.ds(at_least(half * part, LANES), part)]
+        part = block_rows // 2
+        unit_cols = pl.ds(at_least(first, LANES), count * LANES)
+        if half is None:
+            return ref.at[:, unit_cols]
+        return ref.at[pl.ds(at_least(half * part, 16), part), unit_cols]
+
+    def z_start(which, dest):
+        to = lax.rem(dest, 2)
+        sized(which, core, to, lambda n: remote(
+            held(which, y, to, n), place(which, z, y, core, to, n),
+            z_send.at[which, dest], z_recv.at[which, z], {"fs": dest}).start())
+
+    def z_sent(which, dest):
+        to = lax.rem(dest, 2)
+        sized(which, core, to, lambda n: remote(
+            held(which, y, to, n), place(which, z, y, core, to, n),
+            z_send.at[which, dest], z_recv.at[which, z], {"fs": dest}).wait_send())
+
+    def z_pass(which, source):
+        block = place(which, source, y, core, seat, many)
+        return remote(block, block, pass_send.at[which, lax.rem(source, 2)],
+                      z_recv.at[which, source], ZPEER)
+
+    def arrived(which, source):
+        def act(n):
+            block = place(which, source, y, core, seat, n)
+            remote(block, block, y_send.at[which, source], z_recv.at[which, source],
+                   YPEER).wait_recv()
+        sized(which, core, seat, act)
+
+    def across(which, source, step):
+        def act(n):
+            half = 1 - y if step == "recv" else y
+            block = place(which, source, half, core, seat, n)
+            copy = remote(block, block, y_send.at[which, source], y_recv.at[which, source], YPEER)
+            {"start": copy.start, "recv": copy.wait_recv, "send": copy.wait_send}[step]()
+        sized(which, core, seat, act)
+
+    def beside(which, source, half, step, mine=False):
+        slot = 0 if half is None else half
+        whose = 1 - core if step == "recv" else core
+
+        def act(n):
+            block = place(which, source, half, whose, seat, n)
+            start = held(which, half, seat, n) if mine else block
+            copy = remote(start, block, d_send.at[which, source, slot],
+                          d_recv.at[which, source, slot], SIB)
+            {"start": copy.start, "recv": copy.wait_recv, "send": copy.wait_send}[step]()
+        sized(which, whose, seat, act)
+
+    def keep(which, step):
+        def act(n):
+            copy = pltpu.make_async_copy(held(which, None, seat, n),
+                                         place(which, z, None, core, seat, n), own_sem.at[which])
+            {"start": copy.start, "wait": copy.wait}[step]()
+        sized(which, core, seat, act)
+
+    def relay(which, source):
+        arrived(which, source)
+        across(which, source, "start")
+
+    def share(which, source):
+        across(which, source, "recv")
+        beside(which, source, None, "start")
+
+    def feature_cols(owner):
+        return pl.ds(at_least(owner * width, LANES), width)
+
+    def token_rows(half):
+        return pl.ds(at_least(half * rows, 16), rows)
+
+    def stream_copy(number, device, half):
+        return remote(stream.at[token_rows(half), :], rows_all.at[:, feature_cols(lane_id)],
+                      in_send.at[number], in_recv.at[number], device)
+
+    barrier = pltpu.get_barrier_semaphore()
+    greeted = 0
+    for device in (SIB, XPEER, XSIB, YPEER, ZPEER, {"fs": near}, {"fs": far}):
+        pl.semaphore_signal(barrier, inc=1, device_id=device, device_id_type=MESH)
+        greeted += 1
+    pl.semaphore_wait(barrier, greeted)
+
+    for which in (IN, OUT):
+        z_start(which, near)
+        z_start(which, peer)
+        if which == IN:
+            stream_copies = [stream_copy(0, XPEER, core), stream_copy(1, XSIB, 1 - core),
+                             stream_copy(2, SIB, 1 - core)]
+            for copy in stream_copies:
+                copy.start()
+            pool_copy = remote(pool_w, pool_sib, pool_send.at[0], pool_recv.at[0], SIB)
+            scale_copy = remote(scale, scale_sib, pool_send.at[1], pool_recv.at[1], SIB)
+            pool_copy.start()
+            scale_copy.start()
+    for which in range(5):
+        keep(which, "start")
+        if which == DOWN:
+            for half in (0, 1):
+                beside(which, z, half, "start", mine=True)
+        else:
+            beside(which, z, None, "start", mine=True)
+    for which in (GATE, UP):
+        z_start(which, peer)
+    for which in (GATE, UP):
+        z_start(which, far)
+
+    @pl.when(inner)
+    def _():
+        for which in (GATE, UP):
+            z_start(which, near)
+
+    rows_all[:, feature_cols(lane_id)] = stream[token_rows(core), :]
+
+    def take(which):
+        relay(which, peer)
+        for source in (near, far):
+            arrived(which, source)
+
+            @pl.when(inner)
+            def _():
+                z_pass(which, source).start()
+            across(which, source, "start")
+
+    take(IN)
+
+    def norm_into(source, gain, target, first, count):
+        tile = 64
+
+        def body(i, carry):
+            at = pl.ds(at_least(first + i * tile, tile), tile)
+            values = source[at, :].astype(f32)
+            mean = jnp.mean(values * values, axis=-1, keepdims=True)
+            target[at, :] = (values * lax.rsqrt(mean + EPSILON)
+                             * gain[...].astype(f32)).astype(bf16)
+            return carry
+
+        lax.fori_loop(0, count // tile, body, 0)
+
+    for copy in stream_copies:
+        copy.wait()
+    norm_into(rows_all, mix_gain, normed, 0, rows)
+    for source in (peer, near, far):
+        share(IN, source)
+    take(OUT)
+    pool_copy.wait()
+    scale_copy.wait()
+    for source in (z, peer, near, far):
+        beside(IN, source, None, "recv")
+    keep(IN, "wait")
+
+    local_groups, group_dim = pool_w.shape[0], pool_w.shape[1]
+    at_row = lax.broadcasted_iota(jnp.int32, (SEQ, SEQ), 0)
+    at_col = lax.broadcasted_iota(jnp.int32, (SEQ, SEQ), 1)
+    pooled = jnp.dot(normed[...], in_all[...], preferred_element_type=f32).astype(bf16)
+    for g in range(2 * local_groups):
+        owner, place_in = divmod(g, local_groups)
+        group = x * 2 * local_groups + g
+        level = lax.div(4 * group, local_groups * tp)
+        reach = jnp.int32(2)
+        for bit in range(1, 4):
+            reach = jnp.where(level >= bit, jnp.int32(2 << bit), reach)
+        inside = jnp.where((at_col <= at_row) & (at_col > at_row - reach), 1.0, 0.0).astype(bf16)
+        counts = jnp.minimum(at_row + 1, reach).astype(f32)[:, :1]
+        is_own = core == owner
+        cols = slice(g * group_dim, (g + 1) * group_dim)
+        own_cols = slice(place_in * group_dim, (place_in + 1) * group_dim)
+        weight = jnp.where(is_own, pool_w[place_in], pool_sib[place_in])
+        factor = jnp.where(is_own, scale[:, own_cols].astype(f32),
+                           scale_sib[:, own_cols].astype(f32))
+        for s in range(rows // SEQ):
+            at = slice(s * SEQ, (s + 1) * SEQ)
+            part = pooled[at, cols]
+            sums = jnp.dot(inside, part, preferred_element_type=f32)
+            contrast = (sums / counts - part.astype(f32)).astype(bf16)
+            mixed = jnp.dot(contrast, weight, preferred_element_type=f32)
+            group_out[at, cols] = (mixed * factor).astype(bf16)
+
+    for source in (peer, near, far):
+        share(OUT, source)
+    for source in (z, peer, near, far):
+        beside(OUT, source, None, "recv")
+    keep(OUT, "wait")
+
+    def half_cols(owner):
+        return pl.ds(at_least(owner * wide, LANES), wide)
+
+    mix_send[...] = jnp.dot(group_out[...], out_all[:, half_cols(1 - x)],
+                            preferred_element_type=f32).astype(bf16)
+    mix_copy = remote(mix_send, mix_recv, mix_sems.at[0], mix_sems.at[1], XPEER)
+    mix_copy.start()
+    mix_own[...] = jnp.dot(group_out[...], out_all[:, half_cols(x)], preferred_element_type=f32)
+    for which in (GATE, UP):
+        relay(which, peer)
+    mix_copy.wait()
+    mid_rows = pl.ds(at_least(seat * rows, 16), rows)
+    mid_all[mid_rows, half_cols(x)] = (
+        rows_all[:, half_cols(x)].astype(f32) + (mix_own[...] + mix_recv[...].astype(f32))).astype(bf16)
+
+    def mid_copy(number, block, device):
+        view = mid_all.at[pl.ds(at_least(block * rows, 16), rows), half_cols(x)]
+        return remote(view, view, mid_send.at[number], mid_recv.at[number], device)
+
+    to_pair, to_x, to_x_later = mid_copy(0, seat, ZPEER), mid_copy(1, seat, XPEER), mid_copy(2, 1 - seat, XPEER)
+    to_pair.start()
+    to_x.start()
+
+    @pl.when(jnp.logical_not(inner))
+    def _():
+        for which in (GATE, UP):
+            z_start(which, near)
+
+    for which in (GATE, UP):
+        share(which, peer)
+    to_pair.wait_recv()
+    to_x_later.start()
+    for which in (GATE, UP):
+        relay(which, near)
+    to_x.wait_recv()
+    norm_into(mid_all, ffn_gain, normed_ffn, seat * rows, rows)
+    for which in (GATE, UP):
+        share(which, near)
+    z_start(DOWN, peer)
+    z_start(DOWN, near)
+    z_start(DOWN, far)
+    to_x_later.wait_recv()
+    norm_into(mid_all, ffn_gain, normed_ffn, (1 - seat) * rows, rows)
+    for which in (GATE, UP):
+        relay(which, far)
+    for which in (GATE, UP):
+        share(which, far)
+    relay(DOWN, peer)
+    beside(DOWN, peer, y, "start")
+    for which in (GATE, UP):
+        for source in (z, peer, near, far):
+            beside(which, source, None, "recv")
+        keep(which, "wait")
+
+    tile = rows
+
+    def gated(i, carry):
+        at = pl.ds(at_least(i * tile, tile), tile)
+        values = normed_ffn[at, :]
+        gate = jnp.dot(values, gate_all[...], preferred_element_type=f32)
+        up = jnp.dot(values, up_all[...], preferred_element_type=f32)
+        hidden[at, :] = (gate / (1.0 + jnp.exp(-gate)) * up).astype(bf16)
+        return carry
+
+    lax.fori_loop(0, 2 * rows // tile, gated, 0)
+
+    sub = width // 2
+    order = (z, peer, near, far)
+    keeps_early = x == pair
+
+    def is_kept(o):
+        return keeps_early if o < 2 else jnp.logical_not(keeps_early)
+
+    def half_of(turn):
+        return y if turn == 0 else 1 - y
+
+    def column_block(o, turn):
+        at = pl.ds(at_least(order[o] * width + half_of(turn) * sub, LANES), sub)
+        slot = 2 * (o % 2) + turn
+        values = jnp.dot(hidden[...], down_all[:, at], preferred_element_type=f32)
+
+        @pl.when(is_kept(o))
+        def _():
+            ffn_own[slot] = values
+
+        @pl.when(jnp.logical_not(is_kept(o)))
+        def _():
+            ffn_send[slot] = values.astype(bf16)
+            x_copy(slot).start()
+
+    def x_copy(slot):
+        return remote(ffn_send.at[slot], ffn_recv.at[slot], x_send.at[slot], x_recv.at[slot], XPEER)
+
+    def pair_copy(o, turn):
+        quarter, half = lax.rem(order[o], 2), half_of(turn)
+        return remote(pair_send.at[quarter, half], pair_recv.at[quarter, half],
+                      p_send.at[quarter, half], p_recv.at[quarter, half], ZPEER)
+
+    def fold(o, turn):
+        slot = 2 * (o % 2) + turn
+        quarter, half = lax.rem(order[o], 2), half_of(turn)
+
+        @pl.when(is_kept(o))
+        def _():
+            x_copy(slot).wait_recv()
+            theirs = pl.ds(at_least((1 - seat) * rows, 16), rows)
+            pair_send[quarter, half] = (ffn_own[slot, theirs, :]
+                                        + ffn_recv[slot, theirs, :].astype(f32)).astype(bf16)
+            pair_copy(o, turn).start()
+
+    def last_copy(half):
+        return remote(last_send.at[half], last_recv.at[half], l_send.at[half], l_recv.at[half], SIB)
+
+    def settle(o, turn):
+        slot = 2 * (o % 2) + turn
+        quarter, half = lax.rem(order[o], 2), half_of(turn)
+
+        @pl.when(is_kept(o))
+        def _():
+            pair_copy(o, turn).wait_recv()
+            ours = pl.ds(at_least(seat * rows, 16), rows)
+            cols = pl.ds(at_least(order[o] * width + half * sub, LANES), sub)
+            total = (ffn_own[slot, ours, :] + ffn_recv[slot, ours, :].astype(f32)
+                     + pair_recv[quarter, half].astype(f32))
+            value = (mid_all[ours, cols].astype(f32) + total).astype(bf16)
+
+            @pl.when(quarter == core)
+            def _():
+                result[token_rows(core), pl.ds(at_least(half * sub, LANES), sub)] = value
+
+            @pl.when(quarter != core)
+            def _():
+                last_send[half] = value
+                last_copy(half).start()
+
+    def pour(source):
+        across(DOWN, source, "recv")
+        beside(DOWN, source, 1 - y, "start")
+
+    def ready(source, turn):
+        beside(DOWN, source, half_of(turn), "recv")
+
+    pour(peer)
+    keep(DOWN, "wait")
+    for turn in (0, 1):
+        ready(z, turn)
+    for turn in (0, 1):
+        column_block(0, turn)
+    for turn in (0, 1):
+        ready(peer, turn)
+        column_block(1, turn)
+    relay(DOWN, near)
+    beside(DOWN, near, y, "start")
+    for o in (0, 1):
+        for turn in (0, 1):
+            fold(o, turn)
+    pour(near)
+    for turn in (0, 1):
+        ready(near, turn)
+        column_block(2, turn)
+    relay(DOWN, far)
+    beside(DOWN, far, y, "start")
+    ready(far, 0)
+    column_block(3, 0)
+    fold(2, 0)
+    fold(2, 1)
+    pour(far)
+    for o in (0, 1):
+        for turn in (0, 1):
+            settle(o, turn)
+    ready(far, 1)
+    column_block(3, 1)
+    fold(3, 0)
+    fold(3, 1)
+    for o in (2, 3):
+        for turn in (0, 1):
+            settle(o, turn)
+
+    for half in (0, 1):
+        last_copy(half).wait()
+        result[token_rows(1 - core), half * sub:(half + 1) * sub] = last_recv[half]
+
+    for which in range(5):
+        z_sent(which, peer)
+        z_sent(which, near)
+        if which not in (IN, OUT):
+            z_sent(which, far)
+        else:
+            @pl.when(inner)
+            def _():
+                for source in (near, far):
+                    z_pass(which, source).wait_send()
+        for source in (peer, near, far):
+            across(which, source, "send")
+        for source in order:
+            for half in (0, 1) if which == DOWN else (None,):
+                beside(which, source, half, "send", mine=False)
+    for copy in (to_pair, to_x, to_x_later):
+        copy.wait_send()
+    for slot in range(4):
+        x_copy(slot).wait_send()
+    for quarter in (0, 1):
+        for half in (0, 1):
+            remote(pair_send.at[quarter, half], pair_recv.at[quarter, half],
+                   p_send.at[quarter, half], p_recv.at[quarter, half], ZPEER).wait_send()
+
+
+def pairs_fit(sizes, stream, in_weight, pool_weight, out_weight, gate_weight, down_weight):
+    reps, fs, tp = sizes
+    tokens, width = stream.shape
+    return (reps == 2 and fs == 4 and tp == 4 and tokens % (2 * SEQ) == 0
+            and width % (2 * LANES) == 0 and gate_weight.shape[1] % LANES == 0
+            and in_weight.shape[1] % LANES == 0 and in_weight.shape[0] % 32 == 0
+            and out_weight.shape[0] % 32 == 0 and gate_weight.shape[0] % 32 == 0
+            and down_weight.shape[1] == width)
+
+
+def pair_on_device(sizes, stream, in_weight, pool_weight, pool_scale, out_weight,
+                   mix_gain, ffn_gain, gate_weight, up_weight, down_weight):
+    if not pairs_fit(sizes, stream, in_weight, pool_weight, out_weight, gate_weight, down_weight):
+        return ring_on_device(sizes, stream, in_weight, pool_weight, pool_scale, out_weight,
+                              mix_gain, ffn_gain, gate_weight, up_weight, down_weight)
+    reps, fs, tp = sizes
+    tokens, width = stream.shape
+    rows, sub = tokens // 2, width // 2
+    features = width * tp
+    channels = in_weight.shape[1]
+    units = gate_weight.shape[1]
+    bf, f32 = jnp.bfloat16, jnp.float32
+    vmem = pl.BlockSpec(memory_space=pltpu.VMEM)
+    hbm = pl.BlockSpec(memory_space=pl.ANY)
+    dma = pltpu.SemaphoreType.DMA
+    flops = 2 * tokens * (2 * features * channels + 3 * features * units)
+    return pl.pallas_call(
+        functools.partial(pair_kernel, sizes),
+        out_shape=jax.ShapeDtypeStruct(stream.shape, bf),
+        in_specs=[vmem] + [hbm] * 5 + [vmem] * 4,
+        out_specs=vmem,
+        scratch_shapes=[
+            pltpu.VMEM((in_weight.shape[0] * fs, 2 * channels), bf),
+            pltpu.VMEM((2 * out_weight.shape[0], out_weight.shape[1] * fs), bf),
+            pltpu.VMEM((up_weight.shape[0] * fs, units), bf),
+            pltpu.VMEM((gate_weight.shape[0] * fs, units), bf),
+            pltpu.VMEM((units, down_weight.shape[1] * fs), bf),
+            pltpu.VMEM((rows, features), bf),
+            pltpu.VMEM((rows, features), bf),
+            pltpu.VMEM((rows, 2 * channels), bf),
+            pltpu.VMEM((2 * rows, units), bf),
+            pltpu.VMEM((2 * rows, features), bf),
+            pltpu.VMEM((2 * rows, features), bf),
+            pltpu.VMEM(pool_weight.shape, bf),
+            pltpu.VMEM((1, channels), bf),
+            pltpu.VMEM((rows, 2 * width), f32),
+            pltpu.VMEM((rows, 2 * width), bf),
+            pltpu.VMEM((rows, 2 * width), bf),
+            pltpu.VMEM((4, 2 * rows, sub), f32),
+            pltpu.VMEM((4, 2 * rows, sub), bf),
+            pltpu.VMEM((4, 2 * rows, sub), bf),
+            pltpu.VMEM((2, 2, rows, sub), bf),
+            pltpu.VMEM((2, 2, rows, sub), bf),
+            pltpu.VMEM((2, rows, sub), bf),
+            pltpu.VMEM((2, rows, sub), bf),
+            dma((5, fs)), dma((5, fs)), dma((2, 2)), dma((5, fs)), dma((5, fs)),
+            dma((5, fs, 2)), dma((5, fs, 2)), dma((5,)),
+            dma((3,)), dma((3,)), dma((2,)), dma((2,)), dma((2,)), dma((3,)), dma((3,)),
+            dma((4,)), dma((4,)), dma((2, 2)), dma((2, 2)), dma((2,)), dma((2,)),
+        ],
+        compiler_params=pltpu.CompilerParams(
+            collective_id=0, has_side_effects=True, vmem_limit_bytes=64 * 1024 * 1024 - 65536),
+        cost_estimate=pl.CostEstimate(flops=flops, bytes_accessed=flops // 512, transcendentals=0),
+    )(stream, in_weight, out_weight, up_weight, gate_weight, down_weight, pool_weight,
+      pool_scale.reshape(1, -1), mix_gain.reshape(1, -1), ffn_gain.reshape(1, -1))
+
+
 def solution(mesh):
     sizes = tuple(mesh.shape[name] for name in ("rep", "fs", "tp"))
     return jax.shard_map(
-        functools.partial(on_device, sizes),
+        functools.partial(pair_on_device, sizes),
         mesh=mesh,
         in_specs=(
             P(("rep", "fs"), "tp"),

time: 217 us -> 213 us (0.982)
    pallas_call x1, Pallas kernels: 207 us -> 205 us  [pair_on_device(): pl.pallas_call(functools.partial(pair_kernel, sizes), out_shape=jax.Shape...]
where the time goes in v1:
time: 213 us; the launch traced here: 211 us
  Pallas kernels  205 us (96%)
  local copies, waits for them, and re-layouts  5.64 us (3%)
    pallas_call x1, Pallas kernels, pair_on_device(): pl.pallas_call(functools.partial(pair_kernel, sizes), out_shape=jax.Shape...  205 us

profile of v1, /device:TPU:17, one launch (start us, length us, event | category | flops | bytes accessed | tf_op | source)
XLA Modules:
  0.0 210.6 jit_solution(16451487879238768262)
XLA Ops:
  0.0 1.2 reshape.9.scale
  1.2 1.3 reshape.10.mix_gain
  2.5 1.3 reshape.11.ffn_gain
  3.8 205.0 %shard_map.100 = bf16[512,512]{1,0:T(8,128)(2,1)} custom-call(bf16[512,512]{1,0:T(8,128)(2,1)} %stream.1, bf16[512,256]{1,0:T(8,128)(2,1)} %in_w.1, bf16[256,512]{1,0:T(8,128)(2,1)} %out_w.1, bf16[512,1408]{1,0:T(8,128)(2,1)} %up_w.1, bf16[512,1408]{1,0:T(8,128)(2,1)} %gate_w.1, bf16[1408,512]{1,0:T(8,128)(2,1)} %down_w.1, bf16[2,128,128]{2,1,0:T(8,128)(2,1)} %pool_w.1, ...), custom_call_target="tpu_custom_call" | custom-call | flops 9932111872 | bytes 19398656 | tf_op jit(solution)/shard_map/pallas_call | solution.py:857
  208.7 1.9 copy.12

commit v2 on v1

--- a/solution.py
+++ b/solution.py
@@ -342,7 +342,7 @@
 def pair_kernel(sizes, stream, in_w, out_w, up_w, gate_w, down_w, pool_w, scale,
                 mix_gain, ffn_gain, result,
                 in_all, out_all, up_all, gate_all, down_all,
-                rows_all, normed, group_out, hidden, mid_all, normed_ffn,
+                rows_all, normed, group_out, hidden, gate_acts, mid_all, normed_ffn,
                 pool_sib, scale_sib,
                 mix_own, mix_send, mix_recv, ffn_own, ffn_send, ffn_recv, pair_send, pair_recv,
                 last_send, last_recv,
@@ -520,34 +520,39 @@
         greeted += 1
     pl.semaphore_wait(barrier, greeted)
 
-    for which in (IN, OUT):
-        z_start(which, near)
-        z_start(which, peer)
-        if which == IN:
-            stream_copies = [stream_copy(0, XPEER, core), stream_copy(1, XSIB, 1 - core),
-                             stream_copy(2, SIB, 1 - core)]
-            for copy in stream_copies:
-                copy.start()
-            pool_copy = remote(pool_w, pool_sib, pool_send.at[0], pool_recv.at[0], SIB)
-            scale_copy = remote(scale, scale_sib, pool_send.at[1], pool_recv.at[1], SIB)
-            pool_copy.start()
-            scale_copy.start()
-    for which in range(5):
+    outer = jnp.logical_not(inner)
+    z_start(IN, near)
+    z_start(IN, peer)
+    stream_copies = [stream_copy(0, XPEER, core), stream_copy(1, XSIB, 1 - core),
+                     stream_copy(2, SIB, 1 - core)]
+    for copy in stream_copies:
+        copy.start()
+    z_start(OUT, near)
+    z_start(OUT, peer)
+    keep(IN, "start")
+    beside(IN, z, None, "start", mine=True)
+    pool_copy = remote(pool_w, pool_sib, pool_send.at[0], pool_recv.at[0], SIB)
+    scale_copy = remote(scale, scale_sib, pool_send.at[1], pool_recv.at[1], SIB)
+    pool_copy.start()
+    scale_copy.start()
+
+    @pl.when(inner)
+    def _():
+        z_start(GATE, near)
+        z_start(GATE, far)
+        z_start(UP, near)
+
+    @pl.when(outer)
+    def _():
+        z_start(GATE, peer)
+        z_start(GATE, far)
+        z_start(UP, far)
+        z_start(UP, peer)
+
+    for which in (OUT, GATE, UP, DOWN):
         keep(which, "start")
-        if which == DOWN:
-            for half in (0, 1):
-                beside(which, z, half, "start", mine=True)
-        else:
-            beside(which, z, None, "start", mine=True)
-    for which in (GATE, UP):
-        z_start(which, peer)
-    for which in (GATE, UP):
-        z_start(which, far)
-
-    @pl.when(inner)
-    def _():
-        for which in (GATE, UP):
-            z_start(which, near)
+        for half in (0, 1) if which == DOWN else (None,):
+            beside(which, z, half, "start", mine=True)
 
     rows_all[:, feature_cols(lane_id)] = stream[token_rows(core), :]
 
@@ -562,6 +567,10 @@
             across(which, source, "start")
 
     take(IN)
+
+    @pl.when(inner)
+    def _():
+        take(OUT)
 
     def norm_into(source, gain, target, first, count):
         tile = 64
@@ -581,7 +590,11 @@
     norm_into(rows_all, mix_gain, normed, 0, rows)
     for source in (peer, near, far):
         share(IN, source)
-    take(OUT)
+
+    @pl.when(outer)
+    def _():
+        take(OUT)
+
     pool_copy.wait()
     scale_copy.wait()
     for source in (z, peer, near, far):
@@ -629,8 +642,16 @@
     mix_copy = remote(mix_send, mix_recv, mix_sems.at[0], mix_sems.at[1], XPEER)
     mix_copy.start()
     mix_own[...] = jnp.dot(group_out[...], out_all[:, half_cols(x)], preferred_element_type=f32)
-    for which in (GATE, UP):
-        relay(which, peer)
+
+    @pl.when(inner)
+    def _():
+        relay(GATE, peer)
+        relay(GATE, near)
+
+    @pl.when(outer)
+    def _():
+        relay(GATE, far)
+
     mix_copy.wait()
     mid_rows = pl.ds(at_least(seat * rows, 16), rows)
     mid_all[mid_rows, half_cols(x)] = (
@@ -644,51 +665,105 @@
     to_pair.start()
     to_x.start()
 
-    @pl.when(jnp.logical_not(inner))
-    def _():
-        for which in (GATE, UP):
-            z_start(which, near)
-
-    for which in (GATE, UP):
-        share(which, peer)
+    @pl.when(inner)
+    def _():
+        z_start(GATE, peer)
+        z_start(UP, peer)
+        z_start(UP, far)
+        share(GATE, peer)
+        share(GATE, near)
+        relay(UP, peer)
+
+    @pl.when(outer)
+    def _():
+        z_start(GATE, near)
+        z_start(UP, near)
+        share(GATE, far)
+        relay(UP, far)
+        relay(GATE, near)
+
     to_pair.wait_recv()
     to_x_later.start()
-    for which in (GATE, UP):
-        relay(which, near)
+
+    @pl.when(inner)
+    def _():
+        z_start(DOWN, far)
+        z_start(DOWN, near)
+        z_start(DOWN, peer)
+        share(UP, peer)
+        relay(UP, near)
+
+    @pl.when(outer)
+    def _():
+        z_start(DOWN, peer)
+        z_start(DOWN, near)
+        z_start(DOWN, far)
+        share(UP, far)
+
     to_x.wait_recv()
     norm_into(mid_all, ffn_gain, normed_ffn, seat * rows, rows)
-    for which in (GATE, UP):
-        share(which, near)
-    z_start(DOWN, peer)
-    z_start(DOWN, near)
-    z_start(DOWN, far)
+
+    @pl.when(inner)
+    def _():
+        relay(GATE, far)
+        share(UP, near)
+
+    @pl.when(outer)
+    def _():
+        share(GATE, near)
+        relay(GATE, peer)
+
     to_x_later.wait_recv()
     norm_into(mid_all, ffn_gain, normed_ffn, (1 - seat) * rows, rows)
-    for which in (GATE, UP):
-        relay(which, far)
-    for which in (GATE, UP):
-        share(which, far)
-    relay(DOWN, peer)
-    beside(DOWN, peer, y, "start")
-    for which in (GATE, UP):
-        for source in (z, peer, near, far):
-            beside(which, source, None, "recv")
-        keep(which, "wait")
+
+    @pl.when(inner)
+    def _():
+        relay(UP, far)
+        share(GATE, far)
+
+    @pl.when(outer)
+    def _():
+        relay(UP, peer)
+        share(GATE, peer)
+
+    for source in (z, peer, near, far):
+        beside(GATE, source, None, "recv")
+    keep(GATE, "wait")
 
     tile = rows
 
     def gated(i, carry):
         at = pl.ds(at_least(i * tile, tile), tile)
-        values = normed_ffn[at, :]
-        gate = jnp.dot(values, gate_all[...], preferred_element_type=f32)
-        up = jnp.dot(values, up_all[...], preferred_element_type=f32)
-        hidden[at, :] = (gate / (1.0 + jnp.exp(-gate)) * up).astype(bf16)
+        gate = jnp.dot(normed_ffn[at, :], gate_all[...], preferred_element_type=f32)
+        gate_acts[at, :] = gate / (1.0 + jnp.exp(-gate))
         return carry
 
     lax.fori_loop(0, 2 * rows // tile, gated, 0)
 
+    @pl.when(inner)
+    def _():
+        share(UP, far)
+
+    @pl.when(outer)
+    def _():
+        share(UP, peer)
+        relay(UP, near)
+        share(UP, near)
+
+    for source in (z, peer, near, far):
+        beside(UP, source, None, "recv")
+    keep(UP, "wait")
+
+    def raised(i, carry):
+        at = pl.ds(at_least(i * tile, tile), tile)
+        up = jnp.dot(normed_ffn[at, :], up_all[...], preferred_element_type=f32)
+        hidden[at, :] = (gate_acts[at, :] * up).astype(bf16)
+        return carry
+
+    lax.fori_loop(0, 2 * rows // tile, raised, 0)
+
     sub = width // 2
-    order = (z, peer, near, far)
+    order = (z, peer, far, near)
     keeps_early = x == pair
 
     def is_kept(o):
@@ -763,37 +838,39 @@
     def ready(source, turn):
         beside(DOWN, source, half_of(turn), "recv")
 
+    def bring(source):
+        relay(DOWN, source)
+        beside(DOWN, source, y, "start")
+
+    def block(o, turn):
+        ready(order[o], turn)
+        column_block(o, turn)
+
+    keep(DOWN, "wait")
+    block(0, 0)
+    block(0, 1)
+    bring(peer)
+    block(1, 0)
     pour(peer)
-    keep(DOWN, "wait")
-    for turn in (0, 1):
-        ready(z, turn)
-    for turn in (0, 1):
-        column_block(0, turn)
-    for turn in (0, 1):
-        ready(peer, turn)
-        column_block(1, turn)
-    relay(DOWN, near)
-    beside(DOWN, near, y, "start")
-    for o in (0, 1):
-        for turn in (0, 1):
-            fold(o, turn)
+    block(1, 1)
+    bring(far)
+    fold(0, 0)
+    block(2, 0)
+    pour(far)
+    block(2, 1)
+    fold(0, 1)
+    bring(near)
+    fold(1, 0)
+    block(3, 0)
     pour(near)
-    for turn in (0, 1):
-        ready(near, turn)
-        column_block(2, turn)
-    relay(DOWN, far)
-    beside(DOWN, far, y, "start")
-    ready(far, 0)
-    column_block(3, 0)
     fold(2, 0)
+    fold(1, 1)
     fold(2, 1)
-    pour(far)
+    block(3, 1)
+    fold(3, 0)
     for o in (0, 1):
         for turn in (0, 1):
             settle(o, turn)
-    ready(far, 1)
-    column_block(3, 1)
-    fold(3, 0)
     fold(3, 1)
     for o in (2, 3):
         for turn in (0, 1):
@@ -869,6 +946,7 @@
             pltpu.VMEM((rows, features), bf),
             pltpu.VMEM((rows, 2 * channels), bf),
             pltpu.VMEM((2 * rows, units), bf),
+            pltpu.VMEM((2 * rows, units), f32),
             pltpu.VMEM((2 * rows, features), bf),
             pltpu.VMEM((2 * rows, features), bf),
             pltpu.VMEM(pool_weight.shape, bf),

time: 213 us -> 167 us (0.78)
  Pallas kernels: 205 us -> 161 us
    pallas_call x1, Pallas kernels: 205 us -> 161 us  [pair_on_device(): pl.pallas_call(functools.partial(pair_kernel, sizes), out_shape=jax.Shape...]
where the time goes in v2:
time: 167 us; the launch traced here: 166 us
  Pallas kernels  161 us (96%)
  local copies, waits for them, and re-layouts  5.64 us (3%)
    pallas_call x1, Pallas kernels, pair_on_device(): pl.pallas_call(functools.partial(pair_kernel, sizes), out_shape=jax.Shape...  161 us

profile of v2, /device:TPU:17, one launch (start us, length us, event | category | flops | bytes accessed | tf_op | source)
XLA Modules:
  0.0 166.2 jit_solution(17154899529902393337)
XLA Ops:
  0.0 1.2 reshape.9.scale
  1.2 1.3 reshape.10.mix_gain
  2.5 1.3 reshape.11.ffn_gain
  3.8 160.5 %shard_map.100 = bf16[512,512]{1,0:T(8,128)(2,1)} custom-call(bf16[512,512]{1,0:T(8,128)(2,1)} %stream.1, bf16[512,256]{1,0:T(8,128)(2,1)} %in_w.1, bf16[256,512]{1,0:T(8,128)(2,1)} %out_w.1, bf16[512,1408]{1,0:T(8,128)(2,1)} %up_w.1, bf16[512,1408]{1,0:T(8,128)(2,1)} %gate_w.1, bf16[1408,512]{1,0:T(8,128)(2,1)} %down_w.1, bf16[2,128,128]{2,1,0:T(8,128)(2,1)} %pool_w.1, ...), custom_call_target="tpu_custom_call" | custom-call | flops 9932111872 | bytes 19398656 | tf_op jit(solution)/shard_map/pallas_call | solution.py:934
  164.3 1.9 %copy.12 = bf16[512,512]{1,0:T(8,128)(2,1)} copy(bf16[512,512]{1,0:T(8,128)(2,1)} %shard_map.100) | data formatting | bytes 1048576

commit v3 on v2

--- a/solution.py
+++ b/solution.py
@@ -342,7 +342,7 @@
 def pair_kernel(sizes, stream, in_w, out_w, up_w, gate_w, down_w, pool_w, scale,
                 mix_gain, ffn_gain, result,
                 in_all, out_all, up_all, gate_all, down_all,
-                rows_all, normed, group_out, hidden, gate_acts, mid_all, normed_ffn,
+                rows_all, normed, group_out, hidden, gate_acts, up_acts, mid_all, normed_ffn,
                 pool_sib, scale_sib,
                 mix_own, mix_send, mix_recv, ffn_own, ffn_send, ffn_recv, pair_send, pair_recv,
                 last_send, last_recv,
@@ -395,84 +395,85 @@
         def _():
             act(few)
 
-    def place(which, source, half, core_at, seat_at, count):
+    def extent(which):
+        return own[which].shape[1 if which == DOWN else 0]
+
+    def half_span(which, half, part=None):
+        size = extent(which) // 2
+        if half is None:
+            return 0, 2 * size
+        if part is None:
+            return half * size, size
+        return half * size + part * (size // 2), size // 2
+
+    def parts(which):
+        return (0, 1) if which in (UP, DOWN) else (None,)
+
+    def place(which, source, span, core_at, seat_at, count):
         block_rows, block_cols = own[which].shape
         ref = full[which]
+        start, size = span
+        if which == OUT:
+            return ref.at[pl.ds(at_least(core_at * block_rows + start, 16), size),
+                          pl.ds(at_least(source * block_cols, LANES), block_cols)]
         if which == IN:
-            part = block_rows // 2
-            row, size = (source * block_rows, block_rows) if half is None else (
-                source * block_rows + half * part, part)
-            return ref.at[pl.ds(at_least(row, 16), size),
+            return ref.at[pl.ds(at_least(source * block_rows + start, 16), size),
                           pl.ds(at_least(core_at * block_cols, LANES), block_cols)]
-        if which == OUT:
-            part = block_rows // 2
-            row, size = (core_at * block_rows, block_rows) if half is None else (
-                core_at * block_rows + half * part, part)
-            return ref.at[pl.ds(at_least(row, 16), size),
-                          pl.ds(at_least(source * block_cols, LANES), block_cols)]
         first = core_at * jnp.where(seat_at == 0, many, few) * LANES
         if which == DOWN:
-            part = block_cols // 2
-            col, size = (source * block_cols, block_cols) if half is None else (
-                source * block_cols + half * part, part)
             return ref.at[pl.ds(at_least(first, LANES), count * LANES),
-                          pl.ds(at_least(col, LANES), size)]
-        part = block_rows // 2
-        row, size = (source * block_rows, block_rows) if half is None else (
-            source * block_rows + half * part, part)
-        return ref.at[pl.ds(at_least(row, 16), size),
+                          pl.ds(at_least(source * block_cols + start, LANES), size)]
+        return ref.at[pl.ds(at_least(source * block_rows + start, 16), size),
                       pl.ds(at_least(first, LANES), count * LANES)]
 
-    def held(which, half, seat_at, count):
-        block_rows, block_cols = own[which].shape
+    def held(which, span, seat_at, count):
         ref = own[which]
+        start, size = span
         if which in (IN, OUT):
-            if half is None:
-                return ref
-            part = block_rows // 2
-            return ref.at[pl.ds(at_least(half * part, 16), part), :]
+            return ref.at[pl.ds(at_least(start, 16), size), :]
         first = seat_at * jnp.where(core == 0, many, few) * LANES
         if which == DOWN:
-            part = block_cols // 2
-            unit_rows = pl.ds(at_least(first, LANES), count * LANES)
-            if half is None:
-                return ref.at[unit_rows, :]
-            return ref.at[unit_rows, pl.ds(at_least(half * part, LANES), part)]
-        part = block_rows // 2
-        unit_cols = pl.ds(at_least(first, LANES), count * LANES)
-        if half is None:
-            return ref.at[:, unit_cols]
-        return ref.at[pl.ds(at_least(half * part, 16), part), unit_cols]
+            return ref.at[pl.ds(at_least(first, LANES), count * LANES),
+                          pl.ds(at_least(start, LANES), size)]
+        return ref.at[pl.ds(at_least(start, 16), size),
+                      pl.ds(at_least(first, LANES), count * LANES)]
+
+    def z_copies(which, dest, step):
+        to = lax.rem(dest, 2)
+
+        def act(n):
+            for part in parts(which):
+                span, slot = half_span(which, y, part), part or 0
+                copy = remote(held(which, span, to, n), place(which, z, span, core, to, n),
+                              z_send.at[which, dest, slot], z_recv.at[which, z, slot],
+                              {"fs": dest})
+                {"start": copy.start, "send": copy.wait_send}[step]()
+        sized(which, core, to, act)
 
     def z_start(which, dest):
-        to = lax.rem(dest, 2)
-        sized(which, core, to, lambda n: remote(
-            held(which, y, to, n), place(which, z, y, core, to, n),
-            z_send.at[which, dest], z_recv.at[which, z], {"fs": dest}).start())
+        z_copies(which, dest, "start")
 
     def z_sent(which, dest):
-        to = lax.rem(dest, 2)
-        sized(which, core, to, lambda n: remote(
-            held(which, y, to, n), place(which, z, y, core, to, n),
-            z_send.at[which, dest], z_recv.at[which, z], {"fs": dest}).wait_send())
+        z_copies(which, dest, "send")
 
     def z_pass(which, source):
-        block = place(which, source, y, core, seat, many)
+        block = place(which, source, half_span(which, y), core, seat, many)
         return remote(block, block, pass_send.at[which, lax.rem(source, 2)],
-                      z_recv.at[which, source], ZPEER)
-
-    def arrived(which, source):
+                      z_recv.at[which, source, 0], ZPEER)
+
+    def arrived(which, source, part):
         def act(n):
-            block = place(which, source, y, core, seat, n)
-            remote(block, block, y_send.at[which, source], z_recv.at[which, source],
-                   YPEER).wait_recv()
+            block = place(which, source, half_span(which, y, part), core, seat, n)
+            remote(block, block, y_send.at[which, source, part or 0],
+                   z_recv.at[which, source, part or 0], YPEER).wait_recv()
         sized(which, core, seat, act)
 
-    def across(which, source, step):
+    def across(which, source, part, step):
         def act(n):
             half = 1 - y if step == "recv" else y
-            block = place(which, source, half, core, seat, n)
-            copy = remote(block, block, y_send.at[which, source], y_recv.at[which, source], YPEER)
+            block = place(which, source, half_span(which, half, part), core, seat, n)
+            copy = remote(block, block, y_send.at[which, source, part or 0],
+                          y_recv.at[which, source, part or 0], YPEER)
             {"start": copy.start, "recv": copy.wait_recv, "send": copy.wait_send}[step]()
         sized(which, core, seat, act)
 
@@ -481,8 +482,9 @@
         whose = 1 - core if step == "recv" else core
 
         def act(n):
-            block = place(which, source, half, whose, seat, n)
-            start = held(which, half, seat, n) if mine else block
+            span = half_span(which, half)
+            block = place(which, source, span, whose, seat, n)
+            start = held(which, span, seat, n) if mine else block
             copy = remote(start, block, d_send.at[which, source, slot],
                           d_recv.at[which, source, slot], SIB)
             {"start": copy.start, "recv": copy.wait_recv, "send": copy.wait_send}[step]()
@@ -490,17 +492,21 @@
 
     def keep(which, step):
         def act(n):
-            copy = pltpu.make_async_copy(held(which, None, seat, n),
-                                         place(which, z, None, core, seat, n), own_sem.at[which])
+            span = half_span(which, None)
+            copy = pltpu.make_async_copy(held(which, span, seat, n),
+                                         place(which, z, span, core, seat, n), own_sem.at[which])
             {"start": copy.start, "wait": copy.wait}[step]()
         sized(which, core, seat, act)
 
-    def relay(which, source):
-        arrived(which, source)
-        across(which, source, "start")
+    def relay(which, source, only=None):
+        for part in parts(which):
+            if only is None or part == only:
+                arrived(which, source, part)
+                across(which, source, part, "start")
 
     def share(which, source):
-        across(which, source, "recv")
+        for part in parts(which):
+            across(which, source, part, "recv")
         beside(which, source, None, "start")
 
     def feature_cols(owner):
@@ -559,12 +565,12 @@
     def take(which):
         relay(which, peer)
         for source in (near, far):
-            arrived(which, source)
+            arrived(which, source, None)
 
             @pl.when(inner)
             def _():
                 z_pass(which, source).start()
-            across(which, source, "start")
+            across(which, source, None, "start")
 
     take(IN)
 
@@ -673,6 +679,7 @@
         share(GATE, peer)
         share(GATE, near)
         relay(UP, peer)
+        relay(UP, near)
 
     @pl.when(outer)
     def _():
@@ -691,7 +698,6 @@
         z_start(DOWN, near)
         z_start(DOWN, peer)
         share(UP, peer)
-        relay(UP, near)
 
     @pl.when(outer)
     def _():
@@ -699,23 +705,58 @@
         z_start(DOWN, near)
         z_start(DOWN, far)
         share(UP, far)
+        share(GATE, near)
 
     to_x.wait_recv()
     norm_into(mid_all, ffn_gain, normed_ffn, seat * rows, rows)
 
     @pl.when(inner)
     def _():
+        share(UP, near)
         relay(GATE, far)
-        share(UP, near)
 
     @pl.when(outer)
     def _():
-        share(GATE, near)
         relay(GATE, peer)
 
     to_x_later.wait_recv()
     norm_into(mid_all, ffn_gain, normed_ffn, (1 - seat) * rows, rows)
 
+    early = (jnp.where(inner, z, far), jnp.where(inner, peer, near))
+    later = (jnp.where(inner, near, z), jnp.where(inner, far, peer))
+    depth = gate_all.shape[0] // 2
+    early_at = pl.ds(at_least(jnp.where(inner, pair, 1 - pair) * depth, LANES), depth)
+    later_at = pl.ds(at_least(jnp.where(inner, 1 - pair, pair) * depth, LANES), depth)
+    tile = rows
+
+    def by_tiles(body):
+        def step(i, carry):
+            body(pl.ds(at_least(i * tile, tile), tile))
+            return carry
+        lax.fori_loop(0, 2 * rows // tile, step, 0)
+
+    def partial_dot(at, depth_at, weights):
+        return jnp.dot(normed_ffn[at, depth_at], weights[depth_at, :], preferred_element_type=f32)
+
+    def gate_first(at):
+        gate_acts[at, :] = partial_dot(at, early_at, gate_all)
+
+    def gate_second(at):
+        gate = gate_acts[at, :] + partial_dot(at, later_at, gate_all)
+        gate_acts[at, :] = gate / (1.0 + jnp.exp(-gate))
+
+    def up_first(at):
+        up_acts[at, :] = partial_dot(at, early_at, up_all)
+
+    def up_second(at):
+        up = up_acts[at, :] + partial_dot(at, later_at, up_all)
+        hidden[at, :] = (gate_acts[at, :] * up).astype(bf16)
+
+    keep(GATE, "wait")
+    for source in early:
+        beside(GATE, source, None, "recv")
+    by_tiles(gate_first)
+
     @pl.when(inner)
     def _():
         relay(UP, far)
@@ -723,22 +764,22 @@
 
     @pl.when(outer)
     def _():
+        relay(UP, near)
+        share(GATE, peer)
+
+    for source in later:
+        beside(GATE, source, None, "recv")
+    by_tiles(gate_second)
+
+    @pl.when(outer)
+    def _():
+        share(UP, near)
         relay(UP, peer)
-        share(GATE, peer)
-
-    for source in (z, peer, near, far):
-        beside(GATE, source, None, "recv")
-    keep(GATE, "wait")
-
-    tile = rows
-
-    def gated(i, carry):
-        at = pl.ds(at_least(i * tile, tile), tile)
-        gate = jnp.dot(normed_ffn[at, :], gate_all[...], preferred_element_type=f32)
-        gate_acts[at, :] = gate / (1.0 + jnp.exp(-gate))
-        return carry
-
-    lax.fori_loop(0, 2 * rows // tile, gated, 0)
+
+    keep(UP, "wait")
+    for source in early:
+        beside(UP, source, None, "recv")
+    by_tiles(up_first)
 
     @pl.when(inner)
     def _():
@@ -747,20 +788,11 @@
     @pl.when(outer)
     def _():
         share(UP, peer)
-        relay(UP, near)
-        share(UP, near)
-
-    for source in (z, peer, near, far):
+        relay(DOWN, far, 0)
+
+    for source in later:
         beside(UP, source, None, "recv")
-    keep(UP, "wait")
-
-    def raised(i, carry):
-        at = pl.ds(at_least(i * tile, tile), tile)
-        up = jnp.dot(normed_ffn[at, :], up_all[...], preferred_element_type=f32)
-        hidden[at, :] = (gate_acts[at, :] * up).astype(bf16)
-        return carry
-
-    lax.fori_loop(0, 2 * rows // tile, raised, 0)
+    by_tiles(up_second)
 
     sub = width // 2
     order = (z, peer, far, near)
@@ -832,49 +864,79 @@
                 last_copy(half).start()
 
     def pour(source):
-        across(DOWN, source, "recv")
+        for part in parts(DOWN):
+            across(DOWN, source, part, "recv")
         beside(DOWN, source, 1 - y, "start")
 
     def ready(source, turn):
         beside(DOWN, source, half_of(turn), "recv")
 
-    def bring(source):
-        relay(DOWN, source)
-        beside(DOWN, source, y, "start")
+    OWN, PEER, FAR, NEAR = range(4)
+
+    def bring(o, only=None):
+        relay(DOWN, order[o], only)
+        beside(DOWN, order[o], y, "start")
 
     def block(o, turn):
         ready(order[o], turn)
         column_block(o, turn)
 
     keep(DOWN, "wait")
-    block(0, 0)
-    block(0, 1)
-    bring(peer)
-    block(1, 0)
-    pour(peer)
-    block(1, 1)
-    bring(far)
-    fold(0, 0)
-    block(2, 0)
-    pour(far)
-    block(2, 1)
-    fold(0, 1)
-    bring(near)
-    fold(1, 0)
-    block(3, 0)
-    pour(near)
-    fold(2, 0)
-    fold(1, 1)
-    fold(2, 1)
-    block(3, 1)
-    fold(3, 0)
-    for o in (0, 1):
+
+    @pl.when(outer)
+    def _():
+        bring(FAR, 1)
+        block(OWN, 0)
+        block(OWN, 1)
+        bring(PEER)
+        block(FAR, 0)
+        pour(far)
+        block(FAR, 1)
+        bring(NEAR)
+        block(PEER, 0)
+        pour(peer)
+        block(PEER, 1)
+        fold(OWN, 0)
+        block(NEAR, 0)
+        fold(OWN, 1)
+        fold(FAR, 0)
+        fold(FAR, 1)
+        pour(near)
+        block(NEAR, 1)
+        fold(PEER, 0)
+
+    @pl.when(inner)
+    def _():
+        block(OWN, 0)
+        block(OWN, 1)
+        bring(PEER)
+        block(PEER, 0)
+        bring(FAR)
+        pour(peer)
+        block(PEER, 1)
+        fold(OWN, 0)
+        block(FAR, 0)
+        pour(far)
+        block(FAR, 1)
+        fold(OWN, 1)
+        fold(PEER, 0)
+        fold(FAR, 0)
+        bring(NEAR)
+        fold(FAR, 1)
+        block(NEAR, 0)
+        pour(near)
+        block(NEAR, 1)
+
+    fold(PEER, 1)
+    fold(NEAR, 0)
+    for o in (OWN, PEER):
         for turn in (0, 1):
             settle(o, turn)
-    fold(3, 1)
-    for o in (2, 3):
-        for turn in (0, 1):
-            settle(o, turn)
+    for turn in (0, 1):
+        settle(FAR, turn)
+    fold(NEAR, 1)
+    for turn in (0, 1):
+        settle(NEAR, turn)
 
     for half in (0, 1):
         last_copy(half).wait()
@@ -891,7 +953,8 @@
                 for source in (near, far):
                     z_pass(which, source).wait_send()
         for source in (peer, near, far):
-            across(which, source, "send")
+            for part in parts(which):
+                across(which, source, part, "send")
         for source in order:
             for half in (0, 1) if which == DOWN else (None,):
                 beside(which, source, half, "send", mine=False)
@@ -947,6 +1010,7 @@
             pltpu.VMEM((rows, 2 * channels), bf),
             pltpu.VMEM((2 * rows, units), bf),
             pltpu.VMEM((2 * rows, units), f32),
+            pltpu.VMEM((2 * rows, units), f32),
             pltpu.VMEM((2 * rows, features), bf),
             pltpu.VMEM((2 * rows, features), bf),
             pltpu.VMEM(pool_weight.shape, bf),
@@ -961,7 +1025,7 @@
             pltpu.VMEM((2, 2, rows, sub), bf),
             pltpu.VMEM((2, rows, sub), bf),
             pltpu.VMEM((2, rows, sub), bf),
-            dma((5, fs)), dma((5, fs)), dma((2, 2)), dma((5, fs)), dma((5, fs)),
+            dma((5, fs, 2)), dma((5, fs, 2)), dma((2, 2)), dma((5, fs, 2)), dma((5, fs, 2)),
             dma((5, fs, 2)), dma((5, fs, 2)), dma((5,)),
             dma((3,)), dma((3,)), dma((2,)), dma((2,)), dma((2,)), dma((3,)), dma((3,)),
             dma((4,)), dma((4,)), dma((2, 2)), dma((2, 2)), dma((2,)), dma((2,)),

time: 167 us -> 148 us (0.89)
  Pallas kernels: 161 us -> 142 us
    pallas_call x1, Pallas kernels: 161 us -> 142 us  [pair_on_device(): pl.pallas_call(functools.partial(pair_kernel, sizes), out_shape=jax.Shape...]
where the time goes in v3:
time: 148 us
  Pallas kernels  142 us (96%)
  local copies, waits for them, and re-layouts  5.64 us (4%)
    pallas_call x1, Pallas kernels, pair_on_device(): pl.pallas_call(functools.partial(pair_kernel, sizes), out_shape=jax.Shape...  142 us

profile of v3, /device:TPU:17, one launch (start us, length us, event | category | flops | bytes accessed | tf_op | source)
XLA Modules:
  0.0 147.6 jit_solution(12002959320412611407)
XLA Ops:
  0.0 1.2 reshape.9.scale
  1.2 1.3 reshape.10.mix_gain
  2.5 1.3 reshape.11.ffn_gain
  3.8 141.9 %shard_map.100 = bf16[512,512]{1,0:T(8,128)(2,1)} custom-call(bf16[512,512]{1,0:T(8,128)(2,1)} %stream.1, bf16[512,256]{1,0:T(8,128)(2,1)} %in_w.1, bf16[256,512]{1,0:T(8,128)(2,1)} %out_w.1, bf16[512,1408]{1,0:T(8,128)(2,1)} %up_w.1, bf16[512,1408]{1,0:T(8,128)(2,1)} %gate_w.1, bf16[1408,512]{1,0:T(8,128)(2,1)} %down_w.1, bf16[2,128,128]{2,1,0:T(8,128)(2,1)} %pool_w.1, ...), custom_call_target="tpu_custom_call" | custom-call | flops 9932111872 | bytes 19398656 | tf_op jit(solution)/shard_map/pallas_call | solution.py:997
  145.7 1.9 %copy.12 = bf16[512,512]{1,0:T(8,128)(2,1)} copy(bf16[512,512]{1,0:T(8,128)(2,1)} %shard_map.100) | data formatting | bytes 1048576

commit v4 on v3

--- a/solution.py
+++ b/solution.py
@@ -381,17 +381,16 @@
             src_ref=source, dst_ref=target, send_sem=send, recv_sem=recv,
             device_id=device, device_id_type=MESH)
 
-    def sized(which, core_at, seat_at, act):
+    def sized(which, roomy, act):
         if which in (IN, OUT) or few == many:
             act(many)
             return
-        big = core_at == seat_at
-
-        @pl.when(big)
+
+        @pl.when(roomy)
         def _():
             act(many)
 
-        @pl.when(jnp.logical_not(big))
+        @pl.when(jnp.logical_not(roomy))
         def _():
             act(few)
 
@@ -409,7 +408,7 @@
     def parts(which):
         return (0, 1) if which in (UP, DOWN) else (None,)
 
-    def place(which, source, span, core_at, seat_at, count):
+    def place(which, source, span, core_at, count):
         block_rows, block_cols = own[which].shape
         ref = full[which]
         start, size = span
@@ -419,63 +418,63 @@
         if which == IN:
             return ref.at[pl.ds(at_least(source * block_rows + start, 16), size),
                           pl.ds(at_least(core_at * block_cols, LANES), block_cols)]
-        first = core_at * jnp.where(seat_at == 0, many, few) * LANES
+        first = core_at * (count * LANES)
         if which == DOWN:
             return ref.at[pl.ds(at_least(first, LANES), count * LANES),
                           pl.ds(at_least(source * block_cols + start, LANES), size)]
         return ref.at[pl.ds(at_least(source * block_rows + start, 16), size),
                       pl.ds(at_least(first, LANES), count * LANES)]
 
-    def held(which, span, seat_at, count):
+    def held(which, span, roomy, count):
         ref = own[which]
         start, size = span
         if which in (IN, OUT):
             return ref.at[pl.ds(at_least(start, 16), size), :]
-        first = seat_at * jnp.where(core == 0, many, few) * LANES
+        first = jnp.where(roomy, 0, many * LANES)
         if which == DOWN:
             return ref.at[pl.ds(at_least(first, LANES), count * LANES),
                           pl.ds(at_least(start, LANES), size)]
         return ref.at[pl.ds(at_least(start, 16), size),
                       pl.ds(at_least(first, LANES), count * LANES)]
 
-    def z_copies(which, dest, step):
-        to = lax.rem(dest, 2)
+    def z_copies(which, dest, step, only=None):
+        roomy = (dest == 1) | (dest == 2)
 
         def act(n):
-            for part in parts(which):
+            for part in parts(which) if only is None else (only,):
                 span, slot = half_span(which, y, part), part or 0
-                copy = remote(held(which, span, to, n), place(which, z, span, core, to, n),
+                copy = remote(held(which, span, roomy, n), place(which, z, span, core, n),
                               z_send.at[which, dest, slot], z_recv.at[which, z, slot],
                               {"fs": dest})
                 {"start": copy.start, "send": copy.wait_send}[step]()
-        sized(which, core, to, act)
-
-    def z_start(which, dest):
-        z_copies(which, dest, "start")
+        sized(which, roomy, act)
+
+    def z_start(which, dest, only=None):
+        z_copies(which, dest, "start", only)
 
     def z_sent(which, dest):
         z_copies(which, dest, "send")
 
     def z_pass(which, source):
-        block = place(which, source, half_span(which, y), core, seat, many)
+        block = place(which, source, half_span(which, y), core, many)
         return remote(block, block, pass_send.at[which, lax.rem(source, 2)],
                       z_recv.at[which, source, 0], ZPEER)
 
     def arrived(which, source, part):
         def act(n):
-            block = place(which, source, half_span(which, y, part), core, seat, n)
+            block = place(which, source, half_span(which, y, part), core, n)
             remote(block, block, y_send.at[which, source, part or 0],
                    z_recv.at[which, source, part or 0], YPEER).wait_recv()
-        sized(which, core, seat, act)
+        sized(which, inner, act)
 
     def across(which, source, part, step):
         def act(n):
             half = 1 - y if step == "recv" else y
-            block = place(which, source, half_span(which, half, part), core, seat, n)
+            block = place(which, source, half_span(which, half, part), core, n)
             copy = remote(block, block, y_send.at[which, source, part or 0],
                           y_recv.at[which, source, part or 0], YPEER)
             {"start": copy.start, "recv": copy.wait_recv, "send": copy.wait_send}[step]()
-        sized(which, core, seat, act)
+        sized(which, inner, act)
 
     def beside(which, source, half, step, mine=False):
         slot = 0 if half is None else half
@@ -483,20 +482,20 @@
 
         def act(n):
             span = half_span(which, half)
-            block = place(which, source, span, whose, seat, n)
-            start = held(which, span, seat, n) if mine else block
+            block = place(which, source, span, whose, n)
+            start = held(which, span, inner, n) if mine else block
             copy = remote(start, block, d_send.at[which, source, slot],
                           d_recv.at[which, source, slot], SIB)
             {"start": copy.start, "recv": copy.wait_recv, "send": copy.wait_send}[step]()
-        sized(which, whose, seat, act)
+        sized(which, inner, act)
 
     def keep(which, step):
         def act(n):
             span = half_span(which, None)
-            copy = pltpu.make_async_copy(held(which, span, seat, n),
-                                         place(which, z, span, core, seat, n), own_sem.at[which])
+            copy = pltpu.make_async_copy(held(which, span, inner, n),
+                                         place(which, z, span, core, n), own_sem.at[which])
             {"start": copy.start, "wait": copy.wait}[step]()
-        sized(which, core, seat, act)
+        sized(which, inner, act)
 
     def relay(which, source, only=None):
         for part in parts(which):
@@ -586,7 +585,7 @@
             values = source[at, :].astype(f32)
             mean = jnp.mean(values * values, axis=-1, keepdims=True)
             target[at, :] = (values * lax.rsqrt(mean + EPSILON)
-                             * gain[...].astype(f32)).astype(bf16)
+                             * gain[...].astype(f32).reshape(1, -1)).astype(bf16)
             return carry
 
         lax.fori_loop(0, count // tile, body, 0)
@@ -624,8 +623,8 @@
         cols = slice(g * group_dim, (g + 1) * group_dim)
         own_cols = slice(place_in * group_dim, (place_in + 1) * group_dim)
         weight = jnp.where(is_own, pool_w[place_in], pool_sib[place_in])
-        factor = jnp.where(is_own, scale[:, own_cols].astype(f32),
-                           scale_sib[:, own_cols].astype(f32))
+        factor = jnp.where(is_own, scale[own_cols].astype(f32).reshape(1, -1),
+                           scale_sib[own_cols].astype(f32).reshape(1, -1))
         for s in range(rows // SEQ):
             at = slice(s * SEQ, (s + 1) * SEQ)
             part = pooled[at, cols]
@@ -675,7 +674,10 @@
     def _():
         z_start(GATE, peer)
         z_start(UP, peer)
+        z_start(DOWN, near, 0)
         z_start(UP, far)
+        z_start(DOWN, far)
+        z_start(DOWN, near, 1)
         share(GATE, peer)
         share(GATE, near)
         relay(UP, peer)
@@ -694,10 +696,9 @@
 
     @pl.when(inner)
     def _():
-        z_start(DOWN, far)
-        z_start(DOWN, near)
         z_start(DOWN, peer)
         share(UP, peer)
+        relay(DOWN, near, 0)
 
     @pl.when(outer)
     def _():
@@ -722,38 +723,42 @@
     to_x_later.wait_recv()
     norm_into(mid_all, ffn_gain, normed_ffn, (1 - seat) * rows, rows)
 
-    early = (jnp.where(inner, z, far), jnp.where(inner, peer, near))
-    later = (jnp.where(inner, near, z), jnp.where(inner, far, peer))
     depth = gate_all.shape[0] // 2
+    pair_at = pl.ds(at_least(pair * depth, LANES), depth)
+    cross_at = pl.ds(at_least((1 - pair) * depth, LANES), depth)
     early_at = pl.ds(at_least(jnp.where(inner, pair, 1 - pair) * depth, LANES), depth)
     later_at = pl.ds(at_least(jnp.where(inner, 1 - pair, pair) * depth, LANES), depth)
     tile = rows
 
     def by_tiles(body):
-        def step(i, carry):
-            body(pl.ds(at_least(i * tile, tile), tile))
-            return carry
-        lax.fori_loop(0, 2 * rows // tile, step, 0)
-
-    def partial_dot(at, depth_at, weights):
-        return jnp.dot(normed_ffn[at, depth_at], weights[depth_at, :], preferred_element_type=f32)
-
-    def gate_first(at):
-        gate_acts[at, :] = partial_dot(at, early_at, gate_all)
-
-    def gate_second(at):
-        gate = gate_acts[at, :] + partial_dot(at, later_at, gate_all)
-        gate_acts[at, :] = gate / (1.0 + jnp.exp(-gate))
-
-    def up_first(at):
-        up_acts[at, :] = partial_dot(at, early_at, up_all)
-
-    def up_second(at):
-        up = up_acts[at, :] + partial_dot(at, later_at, up_all)
-        hidden[at, :] = (gate_acts[at, :] * up).astype(bf16)
+        def all_tiles(count):
+            wide_units = 2 * count * LANES
+
+            def step(i, carry):
+                body(pl.ds(at_least(i * tile, tile), tile), wide_units)
+                return carry
+            lax.fori_loop(0, 2 * rows // tile, step, 0)
+        sized(UP, inner, all_tiles)
+
+    def partial_dot(at, depth_at, weights, n):
+        return jnp.dot(normed_ffn[at, depth_at], weights[depth_at, :n], preferred_element_type=f32)
+
+    def gate_first(at, n):
+        gate_acts[at, :n] = partial_dot(at, early_at, gate_all, n)
+
+    def gate_second(at, n):
+        gate = gate_acts[at, :n] + partial_dot(at, later_at, gate_all, n)
+        gate_acts[at, :n] = gate / (1.0 + jnp.exp(-gate))
+
+    def up_first(at, n):
+        up_acts[at, :n] = partial_dot(at, pair_at, up_all, n)
+
+    def up_second(at, n):
+        up = up_acts[at, :n] + partial_dot(at, cross_at, up_all, n)
+        hidden[at, :n] = (gate_acts[at, :n] * up).astype(bf16)
 
     keep(GATE, "wait")
-    for source in early:
+    for source in (jnp.where(inner, z, far), jnp.where(inner, peer, near)):
         beside(GATE, source, None, "recv")
     by_tiles(gate_first)
 
@@ -764,22 +769,23 @@
 
     @pl.when(outer)
     def _():
-        relay(UP, near)
+        relay(UP, peer)
         share(GATE, peer)
 
-    for source in later:
+    for source in (jnp.where(inner, near, z), jnp.where(inner, far, peer)):
         beside(GATE, source, None, "recv")
     by_tiles(gate_second)
 
     @pl.when(outer)
     def _():
-        share(UP, near)
-        relay(UP, peer)
+        share(UP, peer)
+        relay(UP, near)
 
     keep(UP, "wait")
-    for source in early:
+    for source in (z, peer):
         beside(UP, source, None, "recv")
     by_tiles(up_first)
+    relay(DOWN, peer)
 
     @pl.when(inner)
     def _():
@@ -787,10 +793,10 @@
 
     @pl.when(outer)
     def _():
-        share(UP, peer)
-        relay(DOWN, far, 0)
-
-    for source in later:
+        share(UP, near)
+
+    beside(DOWN, peer, y, "start")
+    for source in (near, far):
         beside(UP, source, None, "recv")
     by_tiles(up_second)
 
@@ -804,10 +810,10 @@
     def half_of(turn):
         return y if turn == 0 else 1 - y
 
-    def column_block(o, turn):
+    def column_block(o, turn, n):
         at = pl.ds(at_least(order[o] * width + half_of(turn) * sub, LANES), sub)
         slot = 2 * (o % 2) + turn
-        values = jnp.dot(hidden[...], down_all[:, at], preferred_element_type=f32)
+        values = jnp.dot(hidden[:, :n], down_all[:n, at], preferred_element_type=f32)
 
         @pl.when(is_kept(o))
         def _():
@@ -816,10 +822,13 @@
         @pl.when(jnp.logical_not(is_kept(o)))
         def _():
             ffn_send[slot] = values.astype(bf16)
-            x_copy(slot).start()
-
-    def x_copy(slot):
-        return remote(ffn_send.at[slot], ffn_recv.at[slot], x_send.at[slot], x_recv.at[slot], XPEER)
+            x_copy(slot, 0).start()
+            x_copy(slot, 1).start()
+
+    def x_copy(slot, ours):
+        at = pl.ds(at_least((seat if ours else 1 - seat) * rows, 16), rows)
+        return remote(ffn_send.at[slot, at, :], ffn_recv.at[slot, at, :],
+                      x_send.at[slot, ours], x_recv.at[slot, ours], XPEER)
 
     def pair_copy(o, turn):
         quarter, half = lax.rem(order[o], 2), half_of(turn)
@@ -832,7 +841,7 @@
 
         @pl.when(is_kept(o))
         def _():
-            x_copy(slot).wait_recv()
+            x_copy(slot, 0).wait_recv()
             theirs = pl.ds(at_least((1 - seat) * rows, 16), rows)
             pair_send[quarter, half] = (ffn_own[slot, theirs, :]
                                         + ffn_recv[slot, theirs, :].astype(f32)).astype(bf16)
@@ -847,6 +856,7 @@
 
         @pl.when(is_kept(o))
         def _():
+            x_copy(slot, 1).wait_recv()
             pair_copy(o, turn).wait_recv()
             ours = pl.ds(at_least(seat * rows, 16), rows)
             cols = pl.ds(at_least(order[o] * width + half * sub, LANES), sub)
@@ -877,56 +887,52 @@
         relay(DOWN, order[o], only)
         beside(DOWN, order[o], y, "start")
 
-    def block(o, turn):
+    def block(o, turn, count):
         ready(order[o], turn)
-        column_block(o, turn)
+        column_block(o, turn, 2 * count * LANES)
 
     keep(DOWN, "wait")
 
     @pl.when(outer)
     def _():
-        bring(FAR, 1)
-        block(OWN, 0)
-        block(OWN, 1)
-        bring(PEER)
-        block(FAR, 0)
+        block(OWN, 0, few)
+        block(OWN, 1, few)
+        block(PEER, 0, few)
+        pour(peer)
+        bring(FAR)
+        block(PEER, 1, few)
+        block(FAR, 0, few)
+        fold(OWN, 0)
+        bring(NEAR)
         pour(far)
-        block(FAR, 1)
-        bring(NEAR)
-        block(PEER, 0)
-        pour(peer)
-        block(PEER, 1)
-        fold(OWN, 0)
-        block(NEAR, 0)
+        block(FAR, 1, few)
+        block(NEAR, 0, few)
         fold(OWN, 1)
-        fold(FAR, 0)
-        fold(FAR, 1)
+        fold(PEER, 0)
         pour(near)
-        block(NEAR, 1)
-        fold(PEER, 0)
+        block(NEAR, 1, few)
 
     @pl.when(inner)
     def _():
-        block(OWN, 0)
-        block(OWN, 1)
-        bring(PEER)
-        block(PEER, 0)
+        block(OWN, 0, many)
+        block(OWN, 1, many)
+        block(PEER, 0, many)
         bring(FAR)
         pour(peer)
-        block(PEER, 1)
+        block(PEER, 1, many)
+        block(FAR, 0, many)
         fold(OWN, 0)
-        block(FAR, 0)
         pour(far)
-        block(FAR, 1)
+        block(FAR, 1, many)
+        bring(NEAR, 1)
         fold(OWN, 1)
+        block(NEAR, 0, many)
         fold(PEER, 0)
-        fold(FAR, 0)
-        bring(NEAR)
-        fold(FAR, 1)
-        block(NEAR, 0)
         pour(near)
-        block(NEAR, 1)
-
+        block(NEAR, 1, many)
+
+    fold(FAR, 0)
+    fold(FAR, 1)
     fold(PEER, 1)
     fold(NEAR, 0)
     for o in (OWN, PEER):
@@ -961,7 +967,8 @@
     for copy in (to_pair, to_x, to_x_later):
         copy.wait_send()
     for slot in range(4):
-        x_copy(slot).wait_send()
+        for ours in (0, 1):
+            x_copy(slot, ours).wait_send()
     for quarter in (0, 1):
         for half in (0, 1):
             remote(pair_send.at[quarter, half], pair_recv.at[quarter, half],
@@ -988,12 +995,13 @@
     rows, sub = tokens // 2, width // 2
     features = width * tp
     channels = in_weight.shape[1]
-    units = gate_weight.shape[1]
+    blocks = gate_weight.shape[1] // LANES
+    units = 2 * LANES * (blocks - blocks // 2)
     bf, f32 = jnp.bfloat16, jnp.float32
     vmem = pl.BlockSpec(memory_space=pltpu.VMEM)
     hbm = pl.BlockSpec(memory_space=pl.ANY)
     dma = pltpu.SemaphoreType.DMA
-    flops = 2 * tokens * (2 * features * channels + 3 * features * units)
+    flops = 2 * tokens * (2 * features * channels + 3 * features * gate_weight.shape[1])
     return pl.pallas_call(
         functools.partial(pair_kernel, sizes),
         out_shape=jax.ShapeDtypeStruct(stream.shape, bf),
@@ -1014,7 +1022,7 @@
             pltpu.VMEM((2 * rows, features), bf),
             pltpu.VMEM((2 * rows, features), bf),
             pltpu.VMEM(pool_weight.shape, bf),
-            pltpu.VMEM((1, channels), bf),
+            pltpu.VMEM((channels,), bf),
             pltpu.VMEM((rows, 2 * width), f32),
             pltpu.VMEM((rows, 2 * width), bf),
             pltpu.VMEM((rows, 2 * width), bf),
@@ -1028,13 +1036,13 @@
             dma((5, fs, 2)), dma((5, fs, 2)), dma((2, 2)), dma((5, fs, 2)), dma((5, fs, 2)),
             dma((5, fs, 2)), dma((5, fs, 2)), dma((5,)),
             dma((3,)), dma((3,)), dma((2,)), dma((2,)), dma((2,)), dma((3,)), dma((3,)),
-            dma((4,)), dma((4,)), dma((2, 2)), dma((2, 2)), dma((2,)), dma((2,)),
+            dma((4, 2)), dma((4, 2)), dma((2, 2)), dma((2, 2)), dma((2,)), dma((2,)),
         ],
         compiler_params=pltpu.CompilerParams(
             collective_id=0, has_side_effects=True, vmem_limit_bytes=64 * 1024 * 1024 - 65536),
         cost_estimate=pl.CostEstimate(flops=flops, bytes_accessed=flops // 512, transcendentals=0),
     )(stream, in_weight, out_weight, up_weight, gate_weight, down_weight, pool_weight,
-      pool_scale.reshape(1, -1), mix_gain.reshape(1, -1), ffn_gain.reshape(1, -1))
+      pool_scale, mix_gain, ffn_gain)
 
 
 def solution(mesh):

time: 148 us -> 139 us (0.939)
  Pallas kernels: 142 us -> 137 us
  local copies, waits for them, and re-layouts: 5.64 us -> 1.87 us
    pallas_call x1, Pallas kernels: 142 us -> 137 us  [pair_on_device(): pl.pallas_call(functools.partial(pair_kernel, sizes), out_shape=jax.Shape...]
    reshape x3 -> x0, local copies, waits for them, and re-layouts: 3.78 us -> none  [the longest x1 1.29 us: pair_on_device(): mix_gain.reshape(1, -1)]
where the time goes in v4:
time: 139 us
  Pallas kernels  137 us (99%)
  local copies, waits for them, and re-layouts  1.87 us (1%)
    pallas_call x1, Pallas kernels, pair_on_device(): pl.pallas_call(functools.partial(pair_kernel, sizes), out_shape=jax.Shape...  137 us

profile of v4, /device:TPU:17, one launch (start us, length us, event | category | flops | bytes accessed | tf_op | source)
XLA Modules:
  0.0 138.7 jit_solution(1122555238343929102)
XLA Ops:
  0.0 136.8 %shard_map.100 = bf16[512,512]{1,0:T(8,128)(2,1)} custom-call(bf16[512,512]{1,0:T(8,128)(2,1)} %stream.1, bf16[512,256]{1,0:T(8,128)(2,1)} %in_w.1, bf16[256,512]{1,0:T(8,128)(2,1)} %out_w.1, bf16[512,1408]{1,0:T(8,128)(2,1)} %up_w.1, bf16[512,1408]{1,0:T(8,128)(2,1)} %gate_w.1, bf16[1408,512]{1,0:T(8,128)(2,1)} %down_w.1, bf16[2,128,128]{2,1,0:T(8,128)(2,1)} %pool_w.1, ...), custom_call_target="tpu_custom_call" | custom-call | flops 9932111872 | bytes 19398656 | tf_op jit(solution)/shard_map/pallas_call | solution.py:1005
  136.8 1.9 %copy.12 = bf16[512,512]{1,0:T(8,128)(2,1)} copy(bf16[512,512]{1,0:T(8,128)(2,1)} %shard_map.100) | data formatting | bytes 1048576

commit v5 on v4

--- a/solution.py
+++ b/solution.py
@@ -345,10 +345,11 @@
                 rows_all, normed, group_out, hidden, gate_acts, up_acts, mid_all, normed_ffn,
                 pool_sib, scale_sib,
                 mix_own, mix_send, mix_recv, ffn_own, ffn_send, ffn_recv, pair_send, pair_recv,
+                stage, cross_send, cross_recv, cross_own, late_send, late_recv,
                 last_send, last_recv,
                 z_send, z_recv, pass_send, y_send, y_recv, d_send, d_recv, own_sem,
                 in_send, in_recv, pool_send, pool_recv, mix_sems, mid_send, mid_recv,
-                x_send, x_recv, p_send, p_recv, l_send, l_recv):
+                x_send, x_recv, p_send, p_recv, l_send, l_recv, c_send, c_recv, late_sems):
     reps, fs, tp = sizes
     y, z, lane_id = lax.axis_index("rep"), lax.axis_index("fs"), lax.axis_index("tp")
     x, core = lax.div(lane_id, 2), lax.rem(lane_id, 2)
@@ -393,6 +394,22 @@
         @pl.when(jnp.logical_not(roomy))
         def _():
             act(few)
+
+    slot_of = {IN: 0, OUT: 1, GATE: 2, UP: 3, DOWN: 5}
+
+    def role_of(source):
+        return jnp.where(source == peer, 0, jnp.where(source == near, 1,
+                         jnp.where(source == far, 2, 3)))
+
+    def flow(which, part, role):
+        return 3 * (slot_of[which] + (part or 0)) + role
+
+    def beside_flow(which, source, half, part):
+        if which != DOWN:
+            return 4 * (IN, OUT, GATE, UP).index(which) + role_of(source)
+        if source is z:
+            return 16 + half
+        return 18 + 3 * role_of(source) + (0 if part is None else 1 + part)
 
     def extent(which):
         return own[which].shape[1 if which == DOWN else 0]
@@ -442,10 +459,11 @@
 
         def act(n):
             for part in parts(which) if only is None else (only,):
-                span, slot = half_span(which, y, part), part or 0
+                span = half_span(which, y, part)
+                there = jnp.where(dest == peer, 0, jnp.where(inner, 1, 2))
                 copy = remote(held(which, span, roomy, n), place(which, z, span, core, n),
-                              z_send.at[which, dest, slot], z_recv.at[which, z, slot],
-                              {"fs": dest})
+                              z_send.at[flow(which, part, role_of(dest))],
+                              z_recv.at[flow(which, part, there)], {"fs": dest})
                 {"start": copy.start, "send": copy.wait_send}[step]()
         sized(which, roomy, act)
 
@@ -458,34 +476,33 @@
     def z_pass(which, source):
         block = place(which, source, half_span(which, y), core, many)
         return remote(block, block, pass_send.at[which, lax.rem(source, 2)],
-                      z_recv.at[which, source, 0], ZPEER)
+                      z_recv.at[flow(which, None, role_of(source))], ZPEER)
 
     def arrived(which, source, part):
         def act(n):
             block = place(which, source, half_span(which, y, part), core, n)
-            remote(block, block, y_send.at[which, source, part or 0],
-                   z_recv.at[which, source, part or 0], YPEER).wait_recv()
+            at = flow(which, part, role_of(source))
+            remote(block, block, y_send.at[at], z_recv.at[at], YPEER).wait_recv()
         sized(which, inner, act)
 
     def across(which, source, part, step):
         def act(n):
             half = 1 - y if step == "recv" else y
             block = place(which, source, half_span(which, half, part), core, n)
-            copy = remote(block, block, y_send.at[which, source, part or 0],
-                          y_recv.at[which, source, part or 0], YPEER)
+            at = flow(which, part, role_of(source))
+            copy = remote(block, block, y_send.at[at], y_recv.at[at], YPEER)
             {"start": copy.start, "recv": copy.wait_recv, "send": copy.wait_send}[step]()
         sized(which, inner, act)
 
-    def beside(which, source, half, step, mine=False):
-        slot = 0 if half is None else half
+    def beside(which, source, half, step, mine=False, part=None):
+        at = beside_flow(which, source, half, part)
         whose = 1 - core if step == "recv" else core
 
         def act(n):
-            span = half_span(which, half)
+            span = half_span(which, half, part)
             block = place(which, source, span, whose, n)
             start = held(which, span, inner, n) if mine else block
-            copy = remote(start, block, d_send.at[which, source, slot],
-                          d_recv.at[which, source, slot], SIB)
+            copy = remote(start, block, d_send.at[at], d_recv.at[at], SIB)
             {"start": copy.start, "recv": copy.wait_recv, "send": copy.wait_send}[step]()
         sized(which, inner, act)
 
@@ -804,31 +821,73 @@
     order = (z, peer, far, near)
     keeps_early = x == pair
 
-    def is_kept(o):
-        return keeps_early if o < 2 else jnp.logical_not(keeps_early)
-
     def half_of(turn):
         return y if turn == 0 else 1 - y
 
-    def column_block(o, turn, n):
-        at = pl.ds(at_least(order[o] * width + half_of(turn) * sub, LANES), sub)
+    half_sub = sub // 2
+
+    def piece_cols(o, turn, part):
+        start = order[o] * width + half_of(turn) * sub
+        if part is None:
+            return pl.ds(at_least(start, LANES), sub)
+        return pl.ds(at_least(start + part * half_sub, LANES), half_sub)
+
+    def lanes(part):
+        return slice(0, sub) if part is None else slice(part * half_sub, (part + 1) * half_sub)
+
+    ours = pl.ds(at_least(seat * rows, 16), rows)
+    theirs = pl.ds(at_least((1 - seat) * rows, 16), rows)
+
+    OWN, PEER, FAR, NEAR = range(4)
+
+    def kept(o):
+        return keeps_early if o < FAR else jnp.logical_not(keeps_early)
+
+    def column_block(o, turn, part, n):
+        values = jnp.dot(hidden[:, :n], down_all[:n, piece_cols(o, turn, part)],
+                         preferred_element_type=f32)
+        if o == NEAR:
+            stage[:, lanes(part)] = values
+            cross_send[turn, :, lanes(part)] = stage[theirs, lanes(part)].astype(bf16)
+            cross_copy(turn, part).start()
+            cross_own[turn, :, lanes(part)] = stage[ours, lanes(part)]
+            return
         slot = 2 * (o % 2) + turn
-        values = jnp.dot(hidden[:, :n], down_all[:n, at], preferred_element_type=f32)
-
-        @pl.when(is_kept(o))
+
+        @pl.when(kept(o))
         def _():
             ffn_own[slot] = values
 
-        @pl.when(jnp.logical_not(is_kept(o)))
+        @pl.when(jnp.logical_not(kept(o)))
         def _():
             ffn_send[slot] = values.astype(bf16)
             x_copy(slot, 0).start()
             x_copy(slot, 1).start()
 
-    def x_copy(slot, ours):
-        at = pl.ds(at_least((seat if ours else 1 - seat) * rows, 16), rows)
+    def cross_copy(turn, part):
+        at, number = lanes(part), turn + (part or 0)
+        return remote(cross_send.at[turn, :, at], cross_recv.at[turn, :, at],
+                      c_send.at[number], c_recv.at[number], ZPEER)
+
+    def late_copy(turn, part):
+        at, number = lanes(part), turn + (part or 0)
+        return remote(late_send.at[turn, :, at], late_recv.at[turn, :, at],
+                      late_sems.at[0, number], late_sems.at[1, number], XPEER)
+
+    def combine(turn, part=None):
+        at = lanes(part)
+        cross_copy(turn, part).wait_recv()
+
+        @pl.when(keeps_early)
+        def _():
+            late_send[turn, :, at] = (cross_own[turn, :, at]
+                                      + cross_recv[turn, :, at].astype(f32)).astype(bf16)
+            late_copy(turn, part).start()
+
+    def x_copy(slot, mine):
+        at = ours if mine else theirs
         return remote(ffn_send.at[slot, at, :], ffn_recv.at[slot, at, :],
-                      x_send.at[slot, ours], x_recv.at[slot, ours], XPEER)
+                      x_send.at[slot, mine], x_recv.at[slot, mine], XPEER)
 
     def pair_copy(o, turn):
         quarter, half = lax.rem(order[o], 2), half_of(turn)
@@ -839,10 +898,9 @@
         slot = 2 * (o % 2) + turn
         quarter, half = lax.rem(order[o], 2), half_of(turn)
 
-        @pl.when(is_kept(o))
+        @pl.when(kept(o))
         def _():
             x_copy(slot, 0).wait_recv()
-            theirs = pl.ds(at_least((1 - seat) * rows, 16), rows)
             pair_send[quarter, half] = (ffn_own[slot, theirs, :]
                                         + ffn_recv[slot, theirs, :].astype(f32)).astype(bf16)
             pair_copy(o, turn).start()
@@ -850,46 +908,60 @@
     def last_copy(half):
         return remote(last_send.at[half], last_recv.at[half], l_send.at[half], l_recv.at[half], SIB)
 
+    def finish(o, turn, total):
+        quarter, half = lax.rem(order[o], 2), half_of(turn)
+        value = (mid_all[ours, piece_cols(o, turn, None)].astype(f32) + total).astype(bf16)
+
+        @pl.when(quarter == core)
+        def _():
+            result[token_rows(core), pl.ds(at_least(half * sub, LANES), sub)] = value
+
+        @pl.when(quarter != core)
+        def _():
+            last_send[half] = value
+            last_copy(half).start()
+
     def settle(o, turn):
         slot = 2 * (o % 2) + turn
         quarter, half = lax.rem(order[o], 2), half_of(turn)
 
-        @pl.when(is_kept(o))
+        @pl.when(kept(o))
         def _():
-            x_copy(slot, 1).wait_recv()
-            pair_copy(o, turn).wait_recv()
-            ours = pl.ds(at_least(seat * rows, 16), rows)
-            cols = pl.ds(at_least(order[o] * width + half * sub, LANES), sub)
-            total = (ffn_own[slot, ours, :] + ffn_recv[slot, ours, :].astype(f32)
-                     + pair_recv[quarter, half].astype(f32))
-            value = (mid_all[ours, cols].astype(f32) + total).astype(bf16)
-
-            @pl.when(quarter == core)
-            def _():
-                result[token_rows(core), pl.ds(at_least(half * sub, LANES), sub)] = value
-
-            @pl.when(quarter != core)
-            def _():
-                last_send[half] = value
-                last_copy(half).start()
-
-    def pour(source):
+            if o == NEAR:
+                for part in block_parts(o, turn):
+                    late_copy(turn, part).wait_recv()
+                finish(o, turn, cross_own[turn] + cross_recv[turn].astype(f32)
+                       + late_recv[turn].astype(f32))
+            else:
+                x_copy(slot, 1).wait_recv()
+                pair_copy(o, turn).wait_recv()
+                finish(o, turn, ffn_own[slot, ours, :] + ffn_recv[slot, ours, :].astype(f32)
+                       + pair_recv[quarter, half].astype(f32))
+
+    def block_parts(o, turn):
+        return (0, 1) if (o, turn) == (NEAR, 1) else (None,)
+
+    def pour(source, only=None):
         for part in parts(DOWN):
-            across(DOWN, source, part, "recv")
-        beside(DOWN, source, 1 - y, "start")
-
-    def ready(source, turn):
-        beside(DOWN, source, half_of(turn), "recv")
-
-    OWN, PEER, FAR, NEAR = range(4)
+            if only is None or part == only:
+                across(DOWN, source, part, "recv")
+                beside(DOWN, source, 1 - y, "start", part=part)
+
+    def ready(o, turn, only=None):
+        if o == 0 or turn == 0:
+            beside(DOWN, order[o], half_of(turn), "recv")
+            return
+        for part in parts(DOWN):
+            if only is None or part == only:
+                beside(DOWN, order[o], 1 - y, "recv", part=part)
 
     def bring(o, only=None):
         relay(DOWN, order[o], only)
         beside(DOWN, order[o], y, "start")
 
-    def block(o, turn, count):
-        ready(order[o], turn)
-        column_block(o, turn, 2 * count * LANES)
+    def block(o, turn, count, part=None):
+        ready(o, turn, part)
+        column_block(o, turn, part, 2 * count * LANES)
 
     keep(DOWN, "wait")
 
@@ -906,11 +978,14 @@
         bring(NEAR)
         pour(far)
         block(FAR, 1, few)
+        fold(OWN, 1)
         block(NEAR, 0, few)
-        fold(OWN, 1)
+        fold(FAR, 0)
+        pour(near, 0)
+        block(NEAR, 1, few, 0)
         fold(PEER, 0)
-        pour(near)
-        block(NEAR, 1, few)
+        pour(near, 1)
+        block(NEAR, 1, few, 1)
 
     @pl.when(inner)
     def _():
@@ -924,25 +999,24 @@
         fold(OWN, 0)
         pour(far)
         block(FAR, 1, many)
+        fold(OWN, 1)
         bring(NEAR, 1)
-        fold(OWN, 1)
         block(NEAR, 0, many)
+        fold(FAR, 0)
+        pour(near, 0)
+        block(NEAR, 1, many, 0)
         fold(PEER, 0)
-        pour(near)
-        block(NEAR, 1, many)
-
-    fold(FAR, 0)
+        pour(near, 1)
+        block(NEAR, 1, many, 1)
+
     fold(FAR, 1)
+    combine(0)
+    combine(1, 0)
     fold(PEER, 1)
-    fold(NEAR, 0)
-    for o in (OWN, PEER):
+    combine(1, 1)
+    for o in (OWN, FAR, PEER, NEAR):
         for turn in (0, 1):
             settle(o, turn)
-    for turn in (0, 1):
-        settle(FAR, turn)
-    fold(NEAR, 1)
-    for turn in (0, 1):
-        settle(NEAR, turn)
 
     for half in (0, 1):
         last_copy(half).wait()
@@ -961,27 +1035,48 @@
         for source in (peer, near, far):
             for part in parts(which):
                 across(which, source, part, "send")
-        for source in order:
-            for half in (0, 1) if which == DOWN else (None,):
-                beside(which, source, half, "send", mine=False)
+        if which != DOWN:
+            for source in order:
+                beside(which, source, None, "send")
+            continue
+        for half in (0, 1):
+            beside(which, z, half, "send")
+        for source in order[1:]:
+            beside(which, source, y, "send")
+            for part in parts(which):
+                beside(which, source, 1 - y, "send", part=part)
     for copy in (to_pair, to_x, to_x_later):
         copy.wait_send()
-    for slot in range(4):
-        for ours in (0, 1):
-            x_copy(slot, ours).wait_send()
-    for quarter in (0, 1):
-        for half in (0, 1):
-            remote(pair_send.at[quarter, half], pair_recv.at[quarter, half],
-                   p_send.at[quarter, half], p_recv.at[quarter, half], ZPEER).wait_send()
+    near_pieces = [(turn, part) for turn in (0, 1) for part in block_parts(NEAR, turn)]
+    for turn, part in near_pieces:
+        cross_copy(turn, part).wait_send()
+
+    @pl.when(keeps_early)
+    def _():
+        for turn in (0, 1):
+            for mine in (0, 1):
+                x_copy(turn, mine).wait_send()
+            for o in (OWN, PEER):
+                pair_copy(o, turn).wait_send()
+        for turn, part in near_pieces:
+            late_copy(turn, part).wait_send()
+
+    @pl.when(jnp.logical_not(keeps_early))
+    def _():
+        for slot in range(4):
+            for mine in (0, 1):
+                x_copy(slot, mine).wait_send()
+        for turn in (0, 1):
+            pair_copy(FAR, turn).wait_send()
 
 
 def pairs_fit(sizes, stream, in_weight, pool_weight, out_weight, gate_weight, down_weight):
     reps, fs, tp = sizes
     tokens, width = stream.shape
     return (reps == 2 and fs == 4 and tp == 4 and tokens % (2 * SEQ) == 0
-            and width % (2 * LANES) == 0 and gate_weight.shape[1] % LANES == 0
+            and width % (4 * LANES) == 0 and gate_weight.shape[1] % LANES == 0
             and in_weight.shape[1] % LANES == 0 and in_weight.shape[0] % 32 == 0
-            and out_weight.shape[0] % 32 == 0 and gate_weight.shape[0] % 32 == 0
+            and out_weight.shape[0] % 32 == 0 and gate_weight.shape[0] % 64 == 0
             and down_weight.shape[1] == width)
 
 
@@ -1031,12 +1126,19 @@
             pltpu.VMEM((4, 2 * rows, sub), bf),
             pltpu.VMEM((2, 2, rows, sub), bf),
             pltpu.VMEM((2, 2, rows, sub), bf),
+            pltpu.VMEM((2 * rows, sub), f32),
             pltpu.VMEM((2, rows, sub), bf),
             pltpu.VMEM((2, rows, sub), bf),
-            dma((5, fs, 2)), dma((5, fs, 2)), dma((2, 2)), dma((5, fs, 2)), dma((5, fs, 2)),
-            dma((5, fs, 2)), dma((5, fs, 2)), dma((5,)),
+            pltpu.VMEM((2, rows, sub), f32),
+            pltpu.VMEM((2, rows, sub), bf),
+            pltpu.VMEM((2, rows, sub), bf),
+            pltpu.VMEM((2, rows, sub), bf),
+            pltpu.VMEM((2, rows, sub), bf),
+            dma((21,)), dma((21,)), dma((2, 2)), dma((21,)), dma((21,)),
+            dma((27,)), dma((27,)), dma((5,)),
             dma((3,)), dma((3,)), dma((2,)), dma((2,)), dma((2,)), dma((3,)), dma((3,)),
             dma((4, 2)), dma((4, 2)), dma((2, 2)), dma((2, 2)), dma((2,)), dma((2,)),
+            dma((3,)), dma((3,)), dma((2, 3)),
         ],
         compiler_params=pltpu.CompilerParams(
             collective_id=0, has_side_effects=True, vmem_limit_bytes=64 * 1024 * 1024 - 65536),

time: 139 us -> 133 us (0.957)
  Pallas kernels: 137 us -> 130 us
    pallas_call x1, Pallas kernels: 137 us -> 130 us  [pair_on_device(): pl.pallas_call(functools.partial(pair_kernel, sizes), out_shape=jax.Shape...]
where the time goes in v5:
time: 133 us; the launch traced here: 132 us
  Pallas kernels  130 us (98%)
  local copies, waits for them, and re-layouts  1.87 us (1%)
    pallas_call x1, Pallas kernels, pair_on_device(): pl.pallas_call(functools.partial(pair_kernel, sizes), out_shape=jax.Shape...  130 us

profile of v5, /device:TPU:17, one launch (start us, length us, event | category | flops | bytes accessed | tf_op | source)
XLA Modules:
  0.0 131.8 jit_solution(10302659947788020159)
XLA Ops:
  0.0 129.9 %shard_map.100 = bf16[512,512]{1,0:T(8,128)(2,1)} custom-call(bf16[512,512]{1,0:T(8,128)(2,1)} %stream.1, bf16[512,256]{1,0:T(8,128)(2,1)} %in_w.1, bf16[256,512]{1,0:T(8,128)(2,1)} %out_w.1, bf16[512,1408]{1,0:T(8,128)(2,1)} %up_w.1, bf16[512,1408]{1,0:T(8,128)(2,1)} %gate_w.1, bf16[1408,512]{1,0:T(8,128)(2,1)} %down_w.1, bf16[2,128,128]{2,1,0:T(8,128)(2,1)} %pool_w.1, ...), custom_call_target="tpu_custom_call" | custom-call | flops 9932111872 | bytes 19398656 | tf_op jit(solution)/shard_map/pallas_call | solution.py:1100
  129.9 1.9 %copy.12 = bf16[512,512]{1,0:T(8,128)(2,1)} copy(bf16[512,512]{1,0:T(8,128)(2,1)} %shard_map.100) | data formatting | bytes 1048576

commit v6 on v5

--- a/solution.py
+++ b/solution.py
@@ -339,11 +339,11 @@
 LANES = 128
 
 
-def pair_kernel(sizes, stream, in_w, out_w, up_w, gate_w, down_w, pool_w, scale,
-                mix_gain, ffn_gain, result,
+def pair_kernel(sizes, stream, in_w, out_w, up_w, gate_w, down_w, pool_in, scale_in,
+                mix_gain_in, ffn_gain_in, result,
                 in_all, out_all, up_all, gate_all, down_all,
                 rows_all, normed, group_out, hidden, gate_acts, up_acts, mid_all, normed_ffn,
-                pool_sib, scale_sib,
+                pool_w, scale, mix_gain, ffn_gain, pool_sib, scale_sib,
                 mix_own, mix_send, mix_recv, ffn_own, ffn_send, ffn_recv, pair_send, pair_recv,
                 stage, cross_send, cross_recv, cross_own, late_send, late_recv,
                 last_send, last_recv,
@@ -420,12 +420,16 @@
             return 0, 2 * size
         if part is None:
             return half * size, size
-        return half * size + part * (size // 2), size // 2
+        return half * size + min(part, 1) * (size // 2), size // 2
+
+    def unit_rows(part, count):
+        upper = count - count // 2
+        return {1: (0, upper), 2: (upper, count - upper)}.get(part, (0, count))
 
     def parts(which):
-        return (0, 1) if which in (UP, DOWN) else (None,)
-
-    def place(which, source, span, core_at, count):
+        return {UP: (0, 1), DOWN: (0, 1, 2)}.get(which, (None,))
+
+    def place(which, source, span, core_at, count, part=None):
         block_rows, block_cols = own[which].shape
         ref = full[which]
         start, size = span
@@ -437,19 +441,21 @@
                           pl.ds(at_least(core_at * block_cols, LANES), block_cols)]
         first = core_at * (count * LANES)
         if which == DOWN:
-            return ref.at[pl.ds(at_least(first, LANES), count * LANES),
+            skip, taken = unit_rows(part, count)
+            return ref.at[pl.ds(at_least(first + skip * LANES, LANES), taken * LANES),
                           pl.ds(at_least(source * block_cols + start, LANES), size)]
         return ref.at[pl.ds(at_least(source * block_rows + start, 16), size),
                       pl.ds(at_least(first, LANES), count * LANES)]
 
-    def held(which, span, roomy, count):
+    def held(which, span, roomy, count, part=None):
         ref = own[which]
         start, size = span
         if which in (IN, OUT):
             return ref.at[pl.ds(at_least(start, 16), size), :]
         first = jnp.where(roomy, 0, many * LANES)
         if which == DOWN:
-            return ref.at[pl.ds(at_least(first, LANES), count * LANES),
+            skip, taken = unit_rows(part, count)
+            return ref.at[pl.ds(at_least(first + skip * LANES, LANES), taken * LANES),
                           pl.ds(at_least(start, LANES), size)]
         return ref.at[pl.ds(at_least(start, 16), size),
                       pl.ds(at_least(first, LANES), count * LANES)]
@@ -458,10 +464,11 @@
         roomy = (dest == 1) | (dest == 2)
 
         def act(n):
-            for part in parts(which) if only is None else (only,):
+            for part in parts(which) if only is None else only:
                 span = half_span(which, y, part)
                 there = jnp.where(dest == peer, 0, jnp.where(inner, 1, 2))
-                copy = remote(held(which, span, roomy, n), place(which, z, span, core, n),
+                copy = remote(held(which, span, roomy, n, part),
+                              place(which, z, span, core, n, part),
                               z_send.at[flow(which, part, role_of(dest))],
                               z_recv.at[flow(which, part, there)], {"fs": dest})
                 {"start": copy.start, "send": copy.wait_send}[step]()
@@ -480,7 +487,7 @@
 
     def arrived(which, source, part):
         def act(n):
-            block = place(which, source, half_span(which, y, part), core, n)
+            block = place(which, source, half_span(which, y, part), core, n, part)
             at = flow(which, part, role_of(source))
             remote(block, block, y_send.at[at], z_recv.at[at], YPEER).wait_recv()
         sized(which, inner, act)
@@ -488,7 +495,7 @@
     def across(which, source, part, step):
         def act(n):
             half = 1 - y if step == "recv" else y
-            block = place(which, source, half_span(which, half, part), core, n)
+            block = place(which, source, half_span(which, half, part), core, n, part)
             at = flow(which, part, role_of(source))
             copy = remote(block, block, y_send.at[at], y_recv.at[at], YPEER)
             {"start": copy.start, "recv": copy.wait_recv, "send": copy.wait_send}[step]()
@@ -516,7 +523,7 @@
 
     def relay(which, source, only=None):
         for part in parts(which):
-            if only is None or part == only:
+            if only is None or part in only:
                 arrived(which, source, part)
                 across(which, source, part, "start")
 
@@ -534,6 +541,13 @@
     def stream_copy(number, device, half):
         return remote(stream.at[token_rows(half), :], rows_all.at[:, feature_cols(lane_id)],
                       in_send.at[number], in_recv.at[number], device)
+
+    small_copies = [pltpu.make_async_copy(source, target, own_sem.at[6 + number])
+                    for number, (source, target) in enumerate((
+                        (mix_gain_in, mix_gain), (ffn_gain_in, ffn_gain),
+                        (pool_in, pool_w), (scale_in, scale)))]
+    for copy in small_copies:
+        copy.start()
 
     barrier = pltpu.get_barrier_semaphore()
     greeted = 0
@@ -553,8 +567,8 @@
     z_start(OUT, peer)
     keep(IN, "start")
     beside(IN, z, None, "start", mine=True)
-    pool_copy = remote(pool_w, pool_sib, pool_send.at[0], pool_recv.at[0], SIB)
-    scale_copy = remote(scale, scale_sib, pool_send.at[1], pool_recv.at[1], SIB)
+    pool_copy = remote(pool_in, pool_sib, pool_send.at[0], pool_recv.at[0], SIB)
+    scale_copy = remote(scale_in, scale_sib, pool_send.at[1], pool_recv.at[1], SIB)
     pool_copy.start()
     scale_copy.start()
 
@@ -576,7 +590,9 @@
         for half in (0, 1) if which == DOWN else (None,):
             beside(which, z, half, "start", mine=True)
 
-    rows_all[:, feature_cols(lane_id)] = stream[token_rows(core), :]
+    own_rows = pltpu.make_async_copy(stream.at[token_rows(core), :],
+                                     rows_all.at[:, feature_cols(lane_id)], own_sem.at[5])
+    own_rows.start()
 
     def take(which):
         relay(which, peer)
@@ -607,6 +623,9 @@
 
         lax.fori_loop(0, count // tile, body, 0)
 
+    own_rows.wait()
+    for copy in small_copies:
+        copy.wait()
     for copy in stream_copies:
         copy.wait()
     norm_into(rows_all, mix_gain, normed, 0, rows)
@@ -691,10 +710,10 @@
     def _():
         z_start(GATE, peer)
         z_start(UP, peer)
-        z_start(DOWN, near, 0)
+        z_start(DOWN, near, (0,))
         z_start(UP, far)
         z_start(DOWN, far)
-        z_start(DOWN, near, 1)
+        z_start(DOWN, near, (1, 2))
         share(GATE, peer)
         share(GATE, near)
         relay(UP, peer)
@@ -715,7 +734,7 @@
     def _():
         z_start(DOWN, peer)
         share(UP, peer)
-        relay(DOWN, near, 0)
+        relay(DOWN, near, (0,))
 
     @pl.when(outer)
     def _():
@@ -802,6 +821,7 @@
     for source in (z, peer):
         beside(UP, source, None, "recv")
     by_tiles(up_first)
+
     relay(DOWN, peer)
 
     @pl.when(inner)
@@ -813,6 +833,7 @@
         share(UP, near)
 
     beside(DOWN, peer, y, "start")
+
     for source in (near, far):
         beside(UP, source, None, "recv")
     by_tiles(up_second)
@@ -942,16 +963,17 @@
         return (0, 1) if (o, turn) == (NEAR, 1) else (None,)
 
     def pour(source, only=None):
-        for part in parts(DOWN):
+        for part in (0, 1):
             if only is None or part == only:
-                across(DOWN, source, part, "recv")
+                for piece in (0,) if part == 0 else (1, 2):
+                    across(DOWN, source, piece, "recv")
                 beside(DOWN, source, 1 - y, "start", part=part)
 
     def ready(o, turn, only=None):
         if o == 0 or turn == 0:
             beside(DOWN, order[o], half_of(turn), "recv")
             return
-        for part in parts(DOWN):
+        for part in (0, 1):
             if only is None or part == only:
                 beside(DOWN, order[o], 1 - y, "recv", part=part)
 
@@ -971,8 +993,9 @@
         block(OWN, 1, few)
         block(PEER, 0, few)
         pour(peer)
-        bring(FAR)
+        relay(DOWN, far, (0,))
         block(PEER, 1, few)
+        bring(FAR, (1, 2))
         block(FAR, 0, few)
         fold(OWN, 0)
         bring(NEAR)
@@ -998,9 +1021,10 @@
         block(FAR, 0, many)
         fold(OWN, 0)
         pour(far)
+        relay(DOWN, near, (1,))
         block(FAR, 1, many)
         fold(OWN, 1)
-        bring(NEAR, 1)
+        bring(NEAR, (2,))
         block(NEAR, 0, many)
         fold(FAR, 0)
         pour(near, 0)
@@ -1043,7 +1067,7 @@
             beside(which, z, half, "send")
         for source in order[1:]:
             beside(which, source, y, "send")
-            for part in parts(which):
+            for part in (0, 1):
                 beside(which, source, 1 - y, "send", part=part)
     for copy in (to_pair, to_x, to_x_later):
         copy.wait_send()
@@ -1094,13 +1118,13 @@
     units = 2 * LANES * (blocks - blocks // 2)
     bf, f32 = jnp.bfloat16, jnp.float32
     vmem = pl.BlockSpec(memory_space=pltpu.VMEM)
-    hbm = pl.BlockSpec(memory_space=pl.ANY)
+    hbm = pl.BlockSpec(memory_space=pltpu.HBM)
     dma = pltpu.SemaphoreType.DMA
     flops = 2 * tokens * (2 * features * channels + 3 * features * gate_weight.shape[1])
     return pl.pallas_call(
         functools.partial(pair_kernel, sizes),
         out_shape=jax.ShapeDtypeStruct(stream.shape, bf),
-        in_specs=[vmem] + [hbm] * 5 + [vmem] * 4,
+        in_specs=[hbm] * 10,
         out_specs=vmem,
         scratch_shapes=[
             pltpu.VMEM((in_weight.shape[0] * fs, 2 * channels), bf),
@@ -1116,6 +1140,10 @@
             pltpu.VMEM((2 * rows, units), f32),
             pltpu.VMEM((2 * rows, features), bf),
             pltpu.VMEM((2 * rows, features), bf),
+            pltpu.VMEM(pool_weight.shape, bf),
+            pltpu.VMEM((channels,), bf),
+            pltpu.VMEM(mix_gain.shape, bf),
+            pltpu.VMEM(ffn_gain.shape, bf),
             pltpu.VMEM(pool_weight.shape, bf),
             pltpu.VMEM((channels,), bf),
             pltpu.VMEM((rows, 2 * width), f32),
@@ -1134,17 +1162,18 @@
             pltpu.VMEM((2, rows, sub), bf),
             pltpu.VMEM((2, rows, sub), bf),
             pltpu.VMEM((2, rows, sub), bf),
-            dma((21,)), dma((21,)), dma((2, 2)), dma((21,)), dma((21,)),
-            dma((27,)), dma((27,)), dma((5,)),
+            dma((24,)), dma((24,)), dma((2, 2)), dma((24,)), dma((24,)),
+            dma((27,)), dma((27,)), dma((10,)),
             dma((3,)), dma((3,)), dma((2,)), dma((2,)), dma((2,)), dma((3,)), dma((3,)),
             dma((4, 2)), dma((4, 2)), dma((2, 2)), dma((2, 2)), dma((2,)), dma((2,)),
             dma((3,)), dma((3,)), dma((2, 3)),
         ],
         compiler_params=pltpu.CompilerParams(
-            collective_id=0, has_side_effects=True, vmem_limit_bytes=64 * 1024 * 1024 - 65536),
+            collective_id=0, has_side_effects=True, vmem_limit_bytes=52 * 1024 * 1024),
         cost_estimate=pl.CostEstimate(flops=flops, bytes_accessed=flops // 512, transcendentals=0),
-    )(stream, in_weight, out_weight, up_weight, gate_weight, down_weight, pool_weight,
-      pool_scale, mix_gain, ffn_gain)
+    )(*[pltpu.with_memory_space_constraint(v, pltpu.HBM) for v in (
+        stream, in_weight, out_weight, up_weight, gate_weight, down_weight, pool_weight,
+        pool_scale, mix_gain, ffn_gain)])
 
 
 def solution(mesh):

time: 133 us -> 130 us (0.977)
  Pallas kernels: 130 us -> 128 us
    pallas_call x1, Pallas kernels: 130 us -> 128 us  [pair_on_device(): pl.pallas_call(functools.partial(pair_kernel, sizes), out_shape=jax.Shape...]
where the time goes in v6:
time: 130 us; the launch traced here: 129 us
  Pallas kernels  128 us (98%)
    pallas_call x1, Pallas kernels, pair_on_device(): pl.pallas_call(functools.partial(pair_kernel, sizes), out_shape=jax.Shape...  128 us

profile of v6, /device:TPU:17, one launch (start us, length us, event | category | flops | bytes accessed | tf_op | source)
XLA Modules:
  0.0 129.0 jit_solution(10947439335039296882)
XLA Ops:
  0.0 128.2 %shard_map.100 = bf16[512,512]{1,0:T(8,128)(2,1)S(1)} custom-call(bf16[512,512]{1,0:T(8,128)(2,1)} %stream.1, bf16[512,256]{1,0:T(8,128)(2,1)} %in_w.1, bf16[256,512]{1,0:T(8,128)(2,1)} %out_w.1, bf16[512,1408]{1,0:T(8,128)(2,1)} %up_w.1, bf16[512,1408]{1,0:T(8,128)(2,1)} %gate_w.1, bf16[1408,512]{1,0:T(8,128)(2,1)} %down_w.1, bf16[2,128,128]{2,1,0:T(8,128)(2,1)} %pool_in.1, ...), custom_call_target="tpu_custom_call" | custom-call | flops 9932111872 | bytes 19398656 | tf_op jit(solution)/shard_map/pallas_call | solution.py:1124
  128.2 0.8 copy.12

commit v7 on v6

--- a/solution.py
+++ b/solution.py
@@ -867,7 +867,7 @@
     def column_block(o, turn, part, n):
         values = jnp.dot(hidden[:, :n], down_all[:n, piece_cols(o, turn, part)],
                          preferred_element_type=f32)
-        if o == NEAR:
+        if (o, turn) == (NEAR, 1):
             stage[:, lanes(part)] = values
             cross_send[turn, :, lanes(part)] = stage[theirs, lanes(part)].astype(bf16)
             cross_copy(turn, part).start()
@@ -948,7 +948,7 @@
 
         @pl.when(kept(o))
         def _():
-            if o == NEAR:
+            if (o, turn) == (NEAR, 1):
                 for part in block_parts(o, turn):
                     late_copy(turn, part).wait_recv()
                 finish(o, turn, cross_own[turn] + cross_recv[turn].astype(f32)
@@ -1034,9 +1034,9 @@
         block(NEAR, 1, many, 1)
 
     fold(FAR, 1)
-    combine(0)
     combine(1, 0)
     fold(PEER, 1)
+    fold(NEAR, 0)
     combine(1, 1)
     for o in (OWN, FAR, PEER, NEAR):
         for turn in (0, 1):
@@ -1071,15 +1071,16 @@
                 beside(which, source, 1 - y, "send", part=part)
     for copy in (to_pair, to_x, to_x_later):
         copy.wait_send()
-    near_pieces = [(turn, part) for turn in (0, 1) for part in block_parts(NEAR, turn)]
+    near_pieces = [(1, part) for part in block_parts(NEAR, 1)]
     for turn, part in near_pieces:
         cross_copy(turn, part).wait_send()
 
     @pl.when(keeps_early)
     def _():
+        for slot in range(3):
+            for mine in (0, 1):
+                x_copy(slot, mine).wait_send()
         for turn in (0, 1):
-            for mine in (0, 1):
-                x_copy(turn, mine).wait_send()
             for o in (OWN, PEER):
                 pair_copy(o, turn).wait_send()
         for turn, part in near_pieces:
@@ -1090,8 +1091,8 @@
         for slot in range(4):
             for mine in (0, 1):
                 x_copy(slot, mine).wait_send()
-        for turn in (0, 1):
-            pair_copy(FAR, turn).wait_send()
+        for o, turn in ((FAR, 0), (FAR, 1), (NEAR, 0)):
+            pair_copy(o, turn).wait_send()
 
 
 def pairs_fit(sizes, stream, in_weight, pool_weight, out_weight, gate_weight, down_weight):

time: 130 us -> 129 us (level)
  no operation moved by 1% of the time
where the time goes in v7:
time: 129 us; the launch traced here: 128 us
  Pallas kernels  128 us (99%)
    pallas_call x1, Pallas kernels, pair_on_device(): pl.pallas_call(functools.partial(pair_kernel, sizes), out_shape=jax.Shape...  128 us

profile of v7, /device:TPU:17, one launch (start us, length us, event | category | flops | bytes accessed | tf_op | source)
XLA Modules:
  0.0 128.4 jit_solution(9238046607532088891)
XLA Ops:
  0.0 127.6 %shard_map.100 = bf16[512,512]{1,0:T(8,128)(2,1)S(1)} custom-call(bf16[512,512]{1,0:T(8,128)(2,1)} %stream.1, bf16[512,256]{1,0:T(8,128)(2,1)} %in_w.1, bf16[256,512]{1,0:T(8,128)(2,1)} %out_w.1, bf16[512,1408]{1,0:T(8,128)(2,1)} %up_w.1, bf16[512,1408]{1,0:T(8,128)(2,1)} %gate_w.1, bf16[1408,512]{1,0:T(8,128)(2,1)} %down_w.1, bf16[2,128,128]{2,1,0:T(8,128)(2,1)} %pool_in.1, ...), custom_call_target="tpu_custom_call" | custom-call | flops 9932111872 | bytes 19398656 | tf_op jit(solution)/shard_map/pallas_call | solution.py:1125
  127.6 0.8 copy.12

commit v8 on v7

--- a/solution.py
+++ b/solution.py
@@ -489,7 +489,7 @@
         def act(n):
             block = place(which, source, half_span(which, y, part), core, n, part)
             at = flow(which, part, role_of(source))
-            remote(block, block, y_send.at[at], z_recv.at[at], YPEER).wait_recv()
+            remote(block, block, y_send.at[0], z_recv.at[at], YPEER).wait_recv()
         sized(which, inner, act)
 
     def across(which, source, part, step):
@@ -497,7 +497,7 @@
             half = 1 - y if step == "recv" else y
             block = place(which, source, half_span(which, half, part), core, n, part)
             at = flow(which, part, role_of(source))
-            copy = remote(block, block, y_send.at[at], y_recv.at[at], YPEER)
+            copy = remote(block, block, y_send.at[0], y_recv.at[at], YPEER)
             {"start": copy.start, "recv": copy.wait_recv, "send": copy.wait_send}[step]()
         sized(which, inner, act)
 
@@ -1056,9 +1056,6 @@
             def _():
                 for source in (near, far):
                     z_pass(which, source).wait_send()
-        for source in (peer, near, far):
-            for part in parts(which):
-                across(which, source, part, "send")
         if which != DOWN:
             for source in order:
                 beside(which, source, None, "send")
@@ -1069,6 +1066,15 @@
             beside(which, source, y, "send")
             for part in (0, 1):
                 beside(which, source, 1 - y, "send", part=part)
+
+    def forwarded(count):
+        elements = 3 * (in_w.shape[0] * in_w.shape[1] + out_w.shape[0] * out_w.shape[1]
+                        + 2 * gate_w.shape[0] * count * LANES
+                        + down_w.shape[1] * count * LANES) // 2
+        view = down_all.at[pl.ds(0, elements // down_all.shape[1]), :]
+        remote(view, view, y_send.at[0], y_recv.at[0], YPEER).wait_send()
+
+    sized(UP, inner, forwarded)
     for copy in (to_pair, to_x, to_x_later):
         copy.wait_send()
     near_pieces = [(1, part) for part in block_parts(NEAR, 1)]
@@ -1163,7 +1169,7 @@
             pltpu.VMEM((2, rows, sub), bf),
             pltpu.VMEM((2, rows, sub), bf),
             pltpu.VMEM((2, rows, sub), bf),
-            dma((24,)), dma((24,)), dma((2, 2)), dma((24,)), dma((24,)),
+            dma((24,)), dma((24,)), dma((2, 2)), dma((1,)), dma((24,)),
             dma((27,)), dma((27,)), dma((10,)),
             dma((3,)), dma((3,)), dma((2,)), dma((2,)), dma((2,)), dma((3,)), dma((3,)),
             dma((4, 2)), dma((4, 2)), dma((2, 2)), dma((2, 2)), dma((2,)), dma((2,)),

time: 129 us -> 129 us (level)
  no operation moved by 1% of the time
where the time goes in v8:
time: 129 us; the launch traced here: 128 us
  Pallas kernels  127 us (98%)
    pallas_call x1, Pallas kernels, pair_on_device(): pl.pallas_call(functools.partial(pair_kernel, sizes), out_shape=jax.Shape...  127 us

profile of v8, /device:TPU:17, one launch (start us, length us, event | category | flops | bytes accessed | tf_op | source)
XLA Modules:
  0.0 128.2 jit_solution(17837458875245432683)
XLA Ops:
  0.0 127.3 %shard_map.100 = bf16[512,512]{1,0:T(8,128)(2,1)S(1)} custom-call(bf16[512,512]{1,0:T(8,128)(2,1)} %stream.1, bf16[512,256]{1,0:T(8,128)(2,1)} %in_w.1, bf16[256,512]{1,0:T(8,128)(2,1)} %out_w.1, bf16[512,1408]{1,0:T(8,128)(2,1)} %up_w.1, bf16[512,1408]{1,0:T(8,128)(2,1)} %gate_w.1, bf16[1408,512]{1,0:T(8,128)(2,1)} %down_w.1, bf16[2,128,128]{2,1,0:T(8,128)(2,1)} %pool_in.1, ...), custom_call_target="tpu_custom_call" | custom-call | flops 9932111872 | bytes 19398656 | tf_op jit(solution)/shard_map/pallas_call | solution.py:1131
  127.4 0.8 copy.12
